TPU v7x, 128 devices: a whole 4x4x4 slice. The times are simulated.
128 devices in a mesh: ep: 128 (over z, y, x, core).
Axes of the slice: x: 4, y: 4, z: 4, core: 2. Of those that a mesh axis runs over, the one named last changes fastest.
Arguments:
- hidden_in: bfloat16 [256, 2048], P('ep'), may hold values from -6 to 6
- lengths: int32 [256], P('ep'), may hold values from 1 to 1024, as said below
- key_cache: bfloat16 [256, 1024, 512], P('ep'), may hold values from -30 to 30
- value_cache: bfloat16 [256, 1024, 512], P('ep'), may hold values from -6 to 6
- query_w: bfloat16 [2048, 2048], P('ep'), may hold values from -0.125 to 0.125
- key_w: bfloat16 [2048, 512], P('ep'), may hold values from -0.125 to 0.125
- value_w: bfloat16 [2048, 512], P('ep'), may hold values from -0.125 to 0.125
- out_w: bfloat16 [2048, 2048], P('ep'), may hold values from -0.125 to 0.125
- lam_heads: float32 [8], replicated, may hold values from 0.3 to 0.8
- head_gain: float32 [256], replicated, may hold values from 0.1 to 1.9
- attn_gain: float32 [2048], replicated, may hold values from 0.1 to 1.9
- moe_gain: float32 [2048], replicated, may hold values from 0.1 to 1.9
- routing: int32 [256, 6], replicated, may hold values from 0 to 127, all different within a row; in each aligned block of 256 rows (0 to 255, 256 to 511, ...) at most 24 rows name the same one
- route_weight: float32 [256, 6], replicated, may hold values from 0.1 to 0.6
- gate_w: bfloat16 [128, 2048, 512], P('ep'), may hold values from -0.125 to 0.125
- up_w: bfloat16 [128, 2048, 512], P('ep'), may hold values from -0.125 to 0.125
- down_w: bfloat16 [128, 512, 2048], P('ep'), may hold values from -0.25 to 0.25
- shared_gate: bfloat16 [2048, 512], replicated, may hold values from -0.125 to 0.125
- shared_up: bfloat16 [2048, 512], replicated, may hold values from -0.125 to 0.125
- shared_down: bfloat16 [512, 2048], replicated, may hold values from -0.25 to 0.25
Outputs:
- layer_out: bfloat16 [256, 2048], P('ep')
- key_new: bfloat16 [256, 512], P('ep')
- value_new: bfloat16 [256, 512], P('ep')
Inputs may be any that keep to these rules, and one draw needn't show every extreme that they name: `lengths`: some sequence has exactly 1024 positions in use. `routing`: each row names 6 different experts; no expert is named by more than 24 rows, a bound that some block reaches.
All inputs are finite; a program needn't handle non-finite values.
Results may differ from a plain program's by a relative error of at most 0.013.
The roundings to bfloat16 on the way count: a program that leaves them out, or rounds other values in their place, can miss the bound.
Values may be sent and summed in bfloat16 or wider, within the bound.
A program may use at most 64 MiB of HBM per device.

v0:
```python
import jax
import jax.numpy as jnp
from jax import lax
from jax.sharding import Mesh
from jax.sharding import PartitionSpec as P

KV_HEADS = 2
HEAD_DIM = 128
EXP_CAP = 24
EP = ("ep_0", "ep_1", "ep_2", "ep_3")


eps_norm = 1e-06
eps_head = 1e-05
theta_base = 500000.0


def split_up(value, dim, length):
    dims = value.shape
    blocks = value.reshape(*dims[:dim], length, dims[dim] // length, *dims[dim + 1 :])
    return jnp.moveaxis(blocks, dim, 0)


def sent_and_summed(value, axis, dim):
    blocks = split_up(value, dim, lax.axis_size(axis))
    arrived = lax.all_to_all(blocks, axis, split_axis=0, concat_axis=0, tiled=True)
    return arrived.astype(jnp.float32).sum(axis=0)


def summed_rows(value, axes, dim):
    far, near = axes
    blocks = split_up(value, dim, lax.axis_size(far))
    nearer = sent_and_summed(blocks, near, dim + 1)
    arrived = lax.all_to_all(
        nearer.astype(jnp.bfloat16), far, split_axis=0, concat_axis=0, tiled=True
    )
    return arrived.astype(jnp.float32).sum(axis=0)


def rms_scale(row_block, gain_vec, epsilon):
    row_block = row_block.astype(jnp.float32)
    return (
        row_block
        * lax.rsqrt(jnp.mean(row_block * row_block, axis=-1, keepdims=True) + epsilon)
        * gain_vec
    )


def rotate(vectors, positions):
    half_width = vectors.shape[-1] // 2
    inverse = theta_base ** (-jnp.arange(half_width, dtype=jnp.float32) / half_width)
    angles = positions.astype(jnp.float32)[..., None] * inverse
    cosine, sine_part = (jnp.cos(angles), jnp.sin(angles))
    lower_half, upper_half = (vectors[..., :half_width], vectors[..., half_width:])
    return jnp.concatenate(
        [
            lower_half * cosine - upper_half * sine_part,
            lower_half * sine_part + upper_half * cosine,
        ],
        axis=-1,
    )


def attend(queries, key_new, value_new, cache_keys, cache_values, lengths, lam_heads, head_gain):
    num_seqs, kv_heads, group_size = (queries.shape[0], queries.shape[1], queries.shape[2])
    head_dim = queries.shape[-1]
    cache_len = cache_keys.shape[1]
    cache_keys = cache_keys.reshape(num_seqs, cache_len, kv_heads, 2, head_dim)
    cache_values = cache_values.reshape(num_seqs, cache_len, kv_heads, -1)
    value_new = value_new.reshape(num_seqs, kv_heads, -1)
    score_scale = head_dim ** (-0.5)
    scores = (
        jnp.einsum("skgph,sckph->skgpc", queries, cache_keys, preferred_element_type=jnp.float32)
        * score_scale
    )
    self_score = (
        jnp.einsum("skgph,skph->skgp", queries, key_new, preferred_element_type=jnp.float32)
        * score_scale
    )
    live_mask = (jnp.arange(cache_len)[None, :] < lengths[:, None])[:, None, None, None, :]
    peak = jnp.maximum(jnp.max(jnp.where(live_mask, scores, -jnp.inf), axis=-1), self_score)
    weights = jnp.where(live_mask, jnp.exp(scores - peak[..., None]), 0.0)
    self_weight = jnp.exp(self_score - peak)
    totals = jnp.sum(weights, axis=-1) + self_weight
    lambda_grid = lam_heads.reshape(kv_heads, group_size)[None]
    combined = (
        weights[:, :, :, 0] / totals[:, :, :, 0, None]
        - lambda_grid[..., None] * weights[:, :, :, 1] / totals[:, :, :, 1, None]
    ).astype(jnp.bfloat16)
    self_combined = (
        self_weight[..., 0] / totals[..., 0] - lambda_grid * self_weight[..., 1] / totals[..., 1]
    ).astype(jnp.bfloat16)
    head_out = jnp.einsum(
        "skgc,sckv->skgv", combined, cache_values, preferred_element_type=jnp.float32
    )
    head_out = (
        head_out
        + self_combined.astype(jnp.float32)[..., None]
        * value_new.astype(jnp.float32)[:, :, None, :]
    )
    return rms_scale(head_out, head_gain, eps_head).astype(jnp.bfloat16).reshape(num_seqs, -1)


def expert_rows(row_block, routed_here, gate_one, up_one, down_one):
    slot_index = jnp.cumsum(routed_here) - 1
    pick_table = (
        (slot_index[None, :] == jnp.arange(EXP_CAP)[:, None]) & (routed_here[None, :] > 0)
    ).astype(jnp.bfloat16)
    picked = jnp.dot(pick_table, row_block, preferred_element_type=jnp.float32).astype(jnp.bfloat16)
    hidden = (
        jax.nn.silu(jnp.dot(picked, gate_one, preferred_element_type=jnp.float32))
        * jnp.dot(picked, up_one, preferred_element_type=jnp.float32)
    ).astype(jnp.bfloat16)
    result = jnp.dot(hidden, down_one, preferred_element_type=jnp.float32).astype(jnp.bfloat16)
    return jnp.dot(pick_table.T, result, preferred_element_type=jnp.float32)


def on_device(
    hidden_in,
    lengths,
    key_cache,
    value_cache,
    query_w,
    key_w,
    value_w,
    out_w,
    lam_heads,
    head_gain,
    attn_gain,
    moe_gain,
    routing,
    route_weight,
    gate_w,
    up_w,
    down_w,
    shared_gate,
    shared_up,
    shared_down,
):
    devices = lax.axis_size(EP)
    device = lax.axis_index(EP)
    tok_dev = hidden_in.shape[0]
    model_width = hidden_in.shape[1]
    all_rows = lax.all_gather(hidden_in, EP, axis=0, tiled=True)
    normed = rms_scale(all_rows, attn_gain, eps_norm).astype(jnp.bfloat16)
    joined_rows = jnp.concatenate([query_w, key_w, value_w], axis=1)
    column_block = lax.all_to_all(joined_rows, EP, split_axis=1, concat_axis=0, tiled=True)
    column_sums = jnp.dot(normed, column_block, preferred_element_type=jnp.float32)
    projected = lax.all_to_all(column_sums, EP, split_axis=0, concat_axis=1, tiled=True)
    query_cols = query_w.shape[1]
    key_cols = key_w.shape[1]
    queries = rotate(
        projected[:, :query_cols].reshape(tok_dev, KV_HEADS, -1, 2, HEAD_DIM),
        lengths[:, None, None, None],
    ).astype(jnp.bfloat16)
    key_new = rotate(
        projected[:, query_cols : query_cols + key_cols].reshape(tok_dev, KV_HEADS, 2, HEAD_DIM),
        lengths[:, None, None],
    ).astype(jnp.bfloat16)
    value_new = projected[:, query_cols + key_cols :].astype(jnp.bfloat16)
    attn_out = attend(
        queries, key_new, value_new, key_cache, value_cache, lengths, lam_heads, head_gain
    )
    pieces = lax.all_to_all(attn_out, EP, split_axis=1, concat_axis=0, tiled=True)
    routed_here = jnp.sum((routing == device).astype(jnp.int32), axis=1)
    attn_proj = summed_rows(
        jnp.dot(pieces, out_w, preferred_element_type=jnp.float32).astype(jnp.bfloat16),
        (("ep_0", "ep_1", "ep_2"), "ep_3"),
        0,
    ).astype(jnp.bfloat16)
    after_mixer = (hidden_in.astype(jnp.float32) + attn_proj.astype(jnp.float32)).astype(
        jnp.bfloat16
    )
    moe_in = rms_scale(after_mixer, moe_gain, eps_norm).astype(jnp.bfloat16)
    own_routes = lax.dynamic_slice_in_dim(routing, device * tok_dev, tok_dev, 0)
    own_weights = lax.dynamic_slice_in_dim(route_weight, device * tok_dev, tok_dev, 0)
    expert_ids = jnp.arange(devices, dtype=jnp.int32)
    matches = own_routes[:, :, None] == expert_ids[None, None, :]
    chosen = jnp.any(matches, axis=1)
    weight_grid = jnp.sum(jnp.where(matches, own_weights[:, :, None], 0.0), axis=1)
    outgoing = jnp.where(chosen.T[:, :, None], moe_in[None], jnp.zeros((), jnp.bfloat16))
    arrived = lax.all_to_all(outgoing, EP, split_axis=0, concat_axis=0, tiled=True)
    result = expert_rows(
        arrived.reshape(devices * tok_dev, model_width), routed_here, gate_w[0], up_w[0], down_w[0]
    ).astype(jnp.bfloat16)
    returned = lax.all_to_all(
        result.reshape(devices, tok_dev, model_width), EP, split_axis=0, concat_axis=0, tiled=True
    )
    routed = jnp.sum(returned.astype(jnp.float32) * weight_grid.T[:, :, None], axis=0)
    shared_hidden = (
        jax.nn.silu(jnp.dot(moe_in, shared_gate, preferred_element_type=jnp.float32))
        * jnp.dot(moe_in, shared_up, preferred_element_type=jnp.float32)
    ).astype(jnp.bfloat16)
    shared_out = jnp.dot(shared_hidden, shared_down, preferred_element_type=jnp.float32)
    layer_out = (after_mixer.astype(jnp.float32) + routed + shared_out).astype(jnp.bfloat16)
    return (layer_out, key_new.reshape(tok_dev, -1), value_new)


def solution(mesh):
    torus = Mesh(mesh.devices.reshape(4, 4, 4, 2), ("ep_0", "ep_1", "ep_2", "ep_3"))
    return jax.shard_map(
        on_device,
        mesh=torus,
        in_specs=(
            P(EP, None),
            P(EP),
            P(EP, None, None),
            P(EP, None, None),
            P(EP, None),
            P(EP, None),
            P(EP, None),
            P(EP, None),
            P(),
            P(),
            P(),
            P(),
            P(),
            P(),
            P(EP, None, None),
            P(EP, None, None),
            P(EP, None, None),
            P(),
            P(),
            P(),
        ),
        out_specs=(P(EP, None), P(EP, None), P(EP, None)),
        check_vma=False,
    )
```

profile of v0, /device:TPU:0, one launch (start us, length us, event | category | flops | bytes accessed | tf_op | source)
XLA Modules:
  0.0 220.9 jit_solution(17257553948698546519)
XLA Ops:
  7.2 0.7 all-gather.3.cloned.1.call-update
  7.9 0.9 pad_maximum_fusion
  8.8 0.8 all_to_all.52
  9.6 0.3 copy.126
  10.0 1.2 reshape.270
  11.2 11.2 %all-to-all-start = ((bf16[128,2,192]{2,1,0:T(2,128)(2,1)}), bf16[128,2,192]{2,1,0:T(2,128)(2,1)S(1)}, u32[]{:S(2)}, u32[]{:S(2)}) async-start(bf16[128,2,192]{2,1,0:T(2,128)(2,1)} %reshape.270), calls=%async_computation | async-start | bytes 262144 | tf_op jit(solution)/shard_map/all_to_all | solution.py:147
  22.5 9.3 %all-to-all-done = bf16[128,2,192]{2,1,0:T(2,128)(2,1)S(1)} async-done(((bf16[128,2,192]{2,1,0:T(2,128)(2,1)}), bf16[128,2,192]{2,1,0:T(2,128)(2,1)S(1)}, u32[]{:S(2)}, u32[]{:S(2)}) %all-to-all-start) | async-done | bytes 98336 | tf_op jit(solution)/shard_map/all_to_all | solution.py:147
  31.7 1.2 reshape.271
  32.9 44.0 %all-gather.3.cloned.1.call-done = bf16[128,2,2048]{2,1,0:T(2,128)(2,1)} async-done(((bf16[1,2,2048]{2,1,0:T(2,128)(2,1)}), bf16[128,2,2048]{2,1,0:T(2,128)(2,1)}) %all-gather.3.cloned.1.call-update) | async-done | bytes 1048592 | tf_op jit(solution)/shard_map/all_gather | solution.py:144
  76.9 2.5 %reshape.265 = f32[256,2048]{1,0:T(8,128)} reshape(bf16[128,2,2048]{2,1,0:T(2,128)(2,1)} %all-gather.3.cloned.1.call-done) | data formatting | bytes 3145728 | tf_op jit(solution)/shard_map/convert_element_type | solution.py:41
  79.5 2.0 multiply_reduce_fusion.1
  81.4 0.2 copy-done.1
  81.7 0.2 multiply_convert_fusion
  81.9 1.5 dot_general.41
  83.4 2.1 fusion.29
  85.5 0.8 copy.77
  86.3 6.2 %all-to-all-start.1 = ((f32[128,2,24]{2,1,0:T(2,128)}), f32[128,2,24]{2,1,0:T(2,128)S(1)}, u32[]{:S(2)}, u32[]{:S(2)}) async-start(f32[128,2,24]{2,1,0:T(2,128)} %copy.77), calls=%async_computation.1 | async-start | bytes 262144 | tf_op jit(solution)/shard_map/all_to_all | solution.py:149
  92.4 0.1 multiply_cosine_fusion
  92.5 4.0 %reshape.254 = bf16[2,1024,2,2,128]{4,3,2,1,0:T(2,128)(2,1)} reshape(bf16[2,1024,512]{2,1,0:T(8,128)(2,1)} %param.22) | data formatting | bytes 4194304 | tf_op jit(solution)/shard_map/reshape | solution.py:68
  96.5 0.1 mul.265
  96.6 5.2 %all-to-all-done.1 = f32[128,2,24]{2,1,0:T(2,128)S(1)} async-done(((f32[128,2,24]{2,1,0:T(2,128)}), f32[128,2,24]{2,1,0:T(2,128)S(1)}, u32[]{:S(2)}, u32[]{:S(2)}) %all-to-all-start.1) | async-done | bytes 24608 | tf_op jit(solution)/shard_map/all_to_all | solution.py:149
  101.8 0.1 all_to_all.58
  102.0 0.1 fusion.61
  102.2 0.1 fusion.75
  102.3 0.2 fusion.52
  102.5 2.4 %select_reduce_fusion = (f32[2,2,4,2]{2,3,1,0:T(2,128)S(1)}, f32[2,2,4,2,1024]{4,2,3,1,0:T(4,128)S(1)}) fusion(pred[2,1024]{1,0:T(4,128)(4,1)S(1)} %iota_compare_fusion.1, bf16[2,1024,2,2,128]{4,3,2,1,0:T(2,128)(2,1)} %reshape.254, bf16[2,2,4,2,64]{4,2,3,1,0:T(4,128)(2,1)S(1)} %get-tuple-element.8, bf16[2,2,4,2,64]{4,2,3,1,0:T(4,128)(2,1)S(1)} %get-tuple-element.7), kind=kOutput, calls=%fused_computation.31 | convolution fusion | flops 8503264 | bytes 2238592 | tf_op jit(solution)/shard_map/skgph,sckph->skgpc/dot_general | solution.py:73
  104.9 0.2 fusion.60
  105.2 2.1 multiply_reduce_fusion.2
  107.3 0.1 multiply_convert_fusion.1
  107.4 0.1 all_to_all.59
  107.6 14.0 %all_to_all.74 = bf16[2,128,16]{2,0,1:T(2,128)(2,1)S(1)} all-to-all(bf16[2,128,16]{2,0,1:T(2,128)(2,1)S(1)} %copy.84), channel_id=1, replica_groups=mesh['ep_0'=4,'ep_1'=4,'ep_2'=4,'ep_3'=2] {'ep_0','ep_1','ep_2','ep_3'}, dimensions={1} | all-to-all | bytes 16384 | tf_op jit(solution)/shard_map/all_to_all | solution.py:164
  121.5 0.4 convolution_convert_fusion.1
  121.9 1.5 reshape_reshape.3
  123.5 1.9 copy.125
  125.4 4.6 %all_to_all.75 = bf16[2,64,2,2048]{3,2,1,0:T(2,128)(2,1)S(1)} all-to-all(bf16[2,64,2,2048]{3,2,1,0:T(2,128)(2,1)S(1)} %bitcast.97), channel_id=1, replica_groups=mesh['ep_0'=4,'ep_1'=4,'ep_2'=4,'ep_3'=2] {'ep_3'}, dimensions={0} | all-to-all | bytes 2097152 | tf_op jit(solution)/shard_map/all_to_all | solution.py:26
  130.0 3.1 %reduce_sum.90 = bf16[64,2,2048]{2,1,0:T(2,128)(2,1)} reduce(bf16[2,64,2,2048]{3,2,1,0:T(2,128)(2,1)S(1)} %all_to_all.75, bf16[]{:T(256)} %constant.30.clone.1), dimensions={0}, to_apply=%region_4.5 | reduce | flops 262144 | bytes 1572866 | tf_op jit(solution)/shard_map/reduce_sum | solution.py:27
  133.1 5.2 %all-to-all-start.4 = ((bf16[64,2,2048]{2,1,0:T(2,128)(2,1)}), bf16[64,2,2048]{2,1,0:T(2,128)(2,1)S(1)}, u32[]{:S(2)}, u32[]{:S(2)}) async-start(bf16[64,2,2048]{2,1,0:T(2,128)(2,1)} %reduce_sum.90), calls=%async_computation.4 | async-start | bytes 1048576 | tf_op jit(solution)/shard_map/all_to_all | solution.py:34
  138.3 0.1 fusion.47
  138.4 0.1 copy.88
  138.6 13.3 %all-to-all-done.4 = bf16[64,2,2048]{2,1,0:T(2,128)(2,1)S(1)} async-done(((bf16[64,2,2048]{2,1,0:T(2,128)(2,1)}), bf16[64,2,2048]{2,1,0:T(2,128)(2,1)S(1)}, u32[]{:S(2)}, u32[]{:S(2)}) %all-to-all-start.4) | async-done | bytes 524320 | tf_op jit(solution)/shard_map/all_to_all | solution.py:34
  151.9 0.4 reduce_sum.91
  152.4 0.1 fusion.40
  152.5 0.1 fusion.42
  152.6 1.8 broadcast_select_fusion
  154.4 4.6 %all-to-all-start.5 = ((bf16[128,2,2048]{2,1,0:T(2,128)(2,1)}), bf16[128,2,2048]{2,1,0:T(2,128)(2,1)S(1)}, u32[]{:S(2)}, u32[]{:S(2)}) async-start(bf16[128,2,2048]{2,1,0:T(2,128)(2,1)} %broadcast_select_fusion), calls=%async_computation.5 | async-start | bytes 2097152 | tf_op jit(solution)/shard_map/all_to_all | solution.py:182
  159.0 0.3 reduce-window.9
  159.5 0.1 slice_reduce_fusion
  159.7 18.5 %all-to-all-done.5 = bf16[128,2,2048]{2,1,0:T(2,128)(2,1)S(1)} async-done(((bf16[128,2,2048]{2,1,0:T(2,128)(2,1)}), bf16[128,2,2048]{2,1,0:T(2,128)(2,1)S(1)}, u32[]{:S(2)}, u32[]{:S(2)}) %all-to-all-start.5) | async-done | bytes 1048608 | tf_op jit(solution)/shard_map/all_to_all | solution.py:182
  178.2 1.2 reshape.259
  179.4 1.6 convolution_convert_fusion.3
  181.0 2.0 fusion.7
  183.0 0.4 fusion.22
  183.4 0.7 convolution_convert_fusion
  184.1 1.5 reshape.260
  185.6 4.6 %all-to-all-start.6 = ((bf16[128,2,2048]{2,1,0:T(2,128)(2,1)}), bf16[128,2,2048]{2,1,0:T(2,128)(2,1)S(1)}, u32[]{:S(2)}, u32[]{:S(2)}) async-start(bf16[128,2,2048]{2,1,0:T(2,128)(2,1)} %reshape.260), calls=%async_computation.6 | async-start | bytes 2097152 | tf_op jit(solution)/shard_map/all_to_all | solution.py:186
  190.2 0.1 constant_dynamic-slice_fusion
  190.3 0.1 select_reduce_fusion.1
  190.4 0.1 copy.89
  190.5 0.1 maximum_convert_fusion
  190.6 0.6 convert_element_type.114
  191.2 2.0 fusion.62
  193.2 16.2 %all-to-all-done.6 = bf16[128,2,2048]{2,1,0:T(2,128)(2,1)S(1)} async-done(((bf16[128,2,2048]{2,1,0:T(2,128)(2,1)}), bf16[128,2,2048]{2,1,0:T(2,128)(2,1)S(1)}, u32[]{:S(2)}, u32[]{:S(2)}) %all-to-all-start.6) | async-done | bytes 1048608 | tf_op jit(solution)/shard_map/all_to_all | solution.py:186
  209.4 1.1 multiply_reduce_fusion
  210.5 3.6 %fusion = bf16[2,2048]{1,0:T(2,128)(2,1)} fusion(bf16[512,2048]{1,0:T(8,128)(2,1)} %param.39, bf16[2,2048]{1,0:T(2,128)(2,1)S(1)} %fusion.42, bf16[2048,512]{1,0:T(8,128)(2,1)} %param.38, f32[2,2048]{1,0:T(2,128)S(1)} %multiply_reduce_fusion, f32[2,512]{1,0:T(2,128)S(1)} %fusion.62, bf16[2,2048]{1,0:T(2,128)(2,1)S(1)} %reduce_sum.91, ...), kind=kOutput, calls=%fused_computation.5 | convolution fusion | flops 8427520 | bytes 4247552 | tf_op jit(solution)/shard_map/dot_general | solution.py:194
  (51 shorter events, 0.8 us)
Async XLA Ops:
  7.2 176.2 %copy-start = (bf16[1,512,2048]{2,1,0:T(8,128)(2,1)S(1)}, bf16[1,512,2048]{2,1,0:T(8,128)(2,1)}, u32[]{:S(2)}) copy-start(bf16[1,512,2048]{2,1,0:T(8,128)(2,1)} %param.36) | copy-start | bytes 6291460
  7.2 15.2 %copy-start.11 = (s32[2]{0:T(128)S(1)}, s32[2]{0:T(128)}, u32[]{:S(2)}) copy-start(s32[2]{0:T(128)} %param.21) | copy-start | bytes 28
  7.2 69.7 %all-gather.3.cloned.1.call-start = ((), (), s32[]{:S(2)}) async-start(), calls=%async_computation.7 | async-start | bytes 1056768 | tf_op jit(solution)/shard_map/all_gather | solution.py:144
  11.2 20.6 %all-to-all-start = ((bf16[128,2,192]{2,1,0:T(2,128)(2,1)}), bf16[128,2,192]{2,1,0:T(2,128)(2,1)S(1)}, u32[]{:S(2)}, u32[]{:S(2)}) async-start(bf16[128,2,192]{2,1,0:T(2,128)(2,1)} %reshape.270), calls=%async_computation | async-start | bytes 262144 | tf_op jit(solution)/shard_map/all_to_all | solution.py:147
  32.9 48.5 %copy-start.6 = (f32[2048]{0:T(1024)S(1)}, f32[2048]{0:T(1024)}, u32[]{:S(2)}) copy-start(f32[2048]{0:T(1024)} %param.30) | copy-start | bytes 24580
  79.5 2.2 %copy-start.1 = (f32[256,2048]{1,0:T(8,128)S(1)}, f32[256,2048]{1,0:T(8,128)}, u32[]{:S(2)}) copy-start(f32[256,2048]{1,0:T(8,128)} %reshape.265) | copy-start | bytes 6291460
  86.3 15.5 %all-to-all-start.1 = ((f32[128,2,24]{2,1,0:T(2,128)}), f32[128,2,24]{2,1,0:T(2,128)S(1)}, u32[]{:S(2)}, u32[]{:S(2)}) async-start(f32[128,2,24]{2,1,0:T(2,128)} %copy.77), calls=%async_computation.1 | async-start | bytes 262144 | tf_op jit(solution)/shard_map/all_to_all | solution.py:149
  92.5 4.0 %copy-start.12 = (f32[8]{0:T(128)S(1)}, f32[8]{0:T(128)}, u32[]{:S(2)}) copy-start(f32[8]{0:T(128)} %param.28) | copy-start | bytes 100
  102.0 5.3 %copy-start.7 = (bf16[2,512]{1,0:T(2,128)(2,1)}, bf16[2,512]{1,0:T(2,128)(2,1)S(1)}, u32[]{:S(2)}) copy-start(bf16[2,512]{1,0:T(2,128)(2,1)S(1)} %slice.111) | copy-start | bytes 6148
  104.9 2.4 %copy-start.10 = (f32[256]{0:T(256)S(1)}, f32[256]{0:T(256)}, u32[]{:S(2)}) copy-start(f32[256]{0:T(256)} %param.29) | copy-start | bytes 3076
  104.9 16.6 %copy-start.4 = (bf16[16,2048]{1,0:T(8,128)(2,1)S(1)}, bf16[16,2048]{1,0:T(8,128)(2,1)}, u32[]{:S(2)}) copy-start(bf16[16,2048]{1,0:T(8,128)(2,1)} %param.27) | copy-start | bytes 196612
  125.4 12.9 %copy-start.5 = (s32[256,6]{0,1:T(8,128)S(1)}, s32[256,6]{0,1:T(8,128)}, u32[]{:S(2)}) copy-start(s32[256,6]{0,1:T(8,128)} %param.32) | copy-start | bytes 18436
  130.0 22.4 %copy-start.3 = (bf16[2,2048]{1,0:T(2,128)(2,1)S(1)}, bf16[2,2048]{1,0:T(2,128)(2,1)}, u32[]{:S(2)}) copy-start(bf16[2,2048]{1,0:T(2,128)(2,1)} %param.20) | copy-start | bytes 24580
  130.0 22.5 %copy-start.8 = (f32[2048]{0:T(1024)S(1)}, f32[2048]{0:T(1024)}, u32[]{:S(2)}) copy-start(f32[2048]{0:T(1024)} %param.31) | copy-start | bytes 24580
  133.1 18.8 %all-to-all-start.4 = ((bf16[64,2,2048]{2,1,0:T(2,128)(2,1)}), bf16[64,2,2048]{2,1,0:T(2,128)(2,1)S(1)}, u32[]{:S(2)}, u32[]{:S(2)}) async-start(bf16[64,2,2048]{2,1,0:T(2,128)(2,1)} %reduce_sum.90), calls=%async_computation.4 | async-start | bytes 1048576 | tf_op jit(solution)/shard_map/all_to_all | solution.py:34
  154.4 23.8 %all-to-all-start.5 = ((bf16[128,2,2048]{2,1,0:T(2,128)(2,1)}), bf16[128,2,2048]{2,1,0:T(2,128)(2,1)S(1)}, u32[]{:S(2)}, u32[]{:S(2)}) async-start(bf16[128,2,2048]{2,1,0:T(2,128)(2,1)} %broadcast_select_fusion), calls=%async_computation.5 | async-start | bytes 2097152 | tf_op jit(solution)/shard_map/all_to_all | solution.py:182
  179.4 3.6 %copy-start.2 = (bf16[1,2048,512]{2,1,0:T(8,128)(2,1)S(1)}, bf16[1,2048,512]{2,1,0:T(8,128)(2,1)}, u32[]{:S(2)}) copy-start(bf16[1,2048,512]{2,1,0:T(8,128)(2,1)} %param.35) | copy-start | bytes 6291460
  184.1 6.2 %copy-start.9 = (f32[256,6]{0,1:T(8,128)S(1)}, f32[256,6]{0,1:T(8,128)}, u32[]{:S(2)}) copy-start(f32[256,6]{0,1:T(8,128)} %param.33) | copy-start | bytes 18436
  185.6 23.8 %all-to-all-start.6 = ((bf16[128,2,2048]{2,1,0:T(2,128)(2,1)}), bf16[128,2,2048]{2,1,0:T(2,128)(2,1)S(1)}, u32[]{:S(2)}, u32[]{:S(2)}) async-start(bf16[128,2,2048]{2,1,0:T(2,128)(2,1)} %reshape.260), calls=%async_computation.6 | async-start | bytes 2097152 | tf_op jit(solution)/shard_map/all_to_all | solution.py:186
Sparse Core Ops, SparseCore 0:
  10.8 66.0 all-gather.2
where the time goes:
time: 222 us; the launch traced here: 221 us
  waiting for transfers between devices  107 us (48%)
  starting transfers between devices  31.8 us (14%)
  local copies, waits for them, and re-layouts  20.6 us (9%)
  blocking collectives  18.5 us (8%)
  matrix products  17.3 us (8%)
  between operations  14.3 us (6%)
  other arithmetic  11.2 us (5%)
    all_gather x1, waiting for transfers between devices, on_device(): all_rows = lax.all_gather(hidden_in, EP, axis=0, tiled=True)  44 us
    all_to_all x1, waiting for transfers between devices, on_device(): lax.all_to_all(outgoing, EP, split_axis=0, concat_axis=0, tiled=True)  18.5 us
    all_to_all x1, waiting for transfers between devices, on_device(): lax.all_to_all(result.reshape(devices, tok_dev, model_width), EP, split_a...  16.2 us
    all_to_all x1, blocking collectives, on_device(): lax.all_to_all(attn_out, EP, split_axis=1, concat_axis=0, tiled=True)  14 us
    all_to_all x1, waiting for transfers between devices, summed_rows(): lax.all_to_all(nearer.astype(jnp.bfloat16), far, split_axis=0, concat_axi...  13.3 us
    all_to_all x1, starting transfers between devices, on_device(): lax.all_to_all(joined_rows, EP, split_axis=1, concat_axis=0, tiled=True)  11.2 us
    all_to_all x1, waiting for transfers between devices, on_device(): lax.all_to_all(joined_rows, EP, split_axis=1, concat_axis=0, tiled=True)  9.28 us
    all_to_all x1, starting transfers between devices, on_device(): lax.all_to_all(column_sums, EP, split_axis=0, concat_axis=1, tiled=True)  6.15 us
  transfers between devices with their start and end apart: 6, of which 6 were waited for; matrix products, arithmetic and copies ran while one was open for 5% of the time, Pallas kernels for 0%

commit v1 on v0

v1 whole, which is shorter than its diff:
```python
import jax
import jax.numpy as jnp
from jax import lax
from jax.experimental import pallas as pl
from jax.experimental.pallas import tpu as pltpu
from jax.sharding import PartitionSpec as P

F32 = jnp.float32
BF16 = jnp.bfloat16
MESH = pl.DeviceIdType.MESH
ANY = pl.ANY
N = 128
D = 2048
CACHE = 1024
SLOTS = 32
W, O, HID, P1, P2, P3, P4, P5, P6, P7 = range(10)


def dot(a, b):
    return jnp.dot(a, b, preferred_element_type=F32)


def rms(x, gain, eps):
    return x * lax.rsqrt(jnp.mean(x * x, axis=-1, keepdims=True) + eps) * gain


def kernel(
    lengths, hidden, cosine, sine, lam, hgain, again, mgain, routing, rweight,
    qw, kw, vw, ow, kc_h, vc_h, gate_h, up_h, down_h, sg_h, su_h, sd_h,
    out, key_out, val_out,
    wcat, obuf_s, wbuf, obuf, kc, vc, gate, up, down, sg, su, sd,
    hs, hbuf, s1, r1, lhs, part, s2, r2, qscr, kscr, vscr, s3, r3, r4, am, gat, res, racc, s7, r7,
    loc, snd, rcv,
):
    me = lax.axis_index("ep")
    z = me // 32
    plane = me % 32
    y = plane // 8
    xc = me % 8
    row = me // 8
    slab = z * 8 + xc

    def local(src, dst, i):
        return pltpu.make_async_copy(src, dst, loc.at[i])

    locals_ = [
        local(qw, wcat.at[:, pl.ds(0, 2048)], 0),
        local(kw, wcat.at[:, pl.ds(2048, 512)], 1),
        local(vw, wcat.at[:, pl.ds(2560, 512)], 2),
        local(ow, obuf_s, 3),
        local(kc_h, kc, 4),
        local(vc_h, vc, 5),
        local(gate_h.at[0], gate, 6),
        local(up_h.at[0], up, 7),
        local(down_h.at[0], down, 8),
        local(sg_h, sg, 9),
        local(su_h, su, 10),
        local(sd_h.at[:, pl.ds(pl.multiple_of(xc * 256, 256), 256)], sd, 11),
    ]
    for c in locals_:
        c.start()

    barrier = pltpu.get_barrier_semaphore()

    def greet(r, carry):
        pl.semaphore_signal(barrier, inc=1, device_id=((me + r) % N,), device_id_type=MESH)
        return carry

    lax.fori_loop(1, N, greet, 0)

    def remote(src, dst, phase, device):
        return pltpu.make_async_remote_copy(
            src_ref=src, dst_ref=dst, send_sem=snd.at[phase], recv_sem=rcv.at[phase],
            device_id=(device,), device_id_type=MESH,
        )

    def arrived(ref, phase):
        remote(ref, ref, phase, (me + 1) % N).wait_recv()

    def left(ref, phase):
        remote(ref, ref, phase, (me + 1) % N).wait_send()

    h32 = hidden[...].astype(F32)
    normed = rms(h32, again[...], 1e-6).astype(BF16).astype(F32)
    for yy in range(4):
        for zz in range(4):
            s1[yy, :, zz * 128 : zz * 128 + 128] = normed[:, zz * 512 + yy * 128 : zz * 512 + yy * 128 + 128]
    for j in range(8):
        hs[j] = h32[:, j * 256 : j * 256 + 256]

    for c in locals_[:4]:
        c.wait()
    pl.semaphore_wait(barrier, N - 1)

    def send_w(r, carry):
        t = (slab + r) % 32
        col = pl.multiple_of((t % 8) * 384, 128)
        at = pl.multiple_of(slab * 16, 16)
        device = (t // 8) * 32 + y * 8 + t % 8
        remote(wcat.at[:, pl.ds(col, 384)], wbuf.at[pl.ds(at, 16), :], W, device).start()
        return carry

    def send_1(r, carry):
        t = (plane + r) % 32
        remote(s1.at[t // 8], r1.at[plane], P1, z * 32 + t).start()
        return carry

    def send_h(r, carry):
        t = (xc + r) % 8
        remote(hs.at[t], hbuf.at[xc], HID, row * 8 + t).start()
        return carry

    def send_o(r, carry):
        t = (slab + r) % 32
        col = pl.multiple_of((t % 8) * 256, 128)
        at = pl.multiple_of(slab * 16, 16)
        device = (t // 8) * 32 + y * 8 + t % 8
        remote(obuf_s.at[:, pl.ds(col, 256)], obuf.at[pl.ds(at, 16), :], O, device).start()
        return carry

    lax.fori_loop(1, 32, send_1, 0)
    lax.fori_loop(1, 32, send_w, 0)
    lax.fori_loop(1, 8, send_h, 0)
    lax.fori_loop(1, 32, send_o, 0)

    own = pl.ds(pl.multiple_of(slab * 16, 16), 16)
    wbuf[own, :] = wcat[:, pl.ds(pl.multiple_of(xc * 384, 128), 384)]
    obuf[own, :] = obuf_s[:, pl.ds(pl.multiple_of(xc * 256, 128), 256)]
    r1[plane] = s1[y]
    hbuf[xc] = hs[xc]

    routed = routing[...] == me
    wcol = jnp.sum(jnp.where(routed, rweight[...], 0.0), axis=1, keepdims=True)
    here = jnp.sum(jnp.where(routed, 1.0, 0.0), axis=1, keepdims=True)
    here = jnp.broadcast_to(here, (256, 128))
    before = lax.broadcasted_iota(jnp.int32, (256, 256), 1) < lax.broadcasted_iota(jnp.int32, (256, 256), 0)
    rank = dot(jnp.where(before, 1.0, 0.0).astype(BF16), here.astype(BF16))
    slot = lax.broadcasted_iota(jnp.int32, (256, 128), 1).astype(F32)
    back = jnp.where(rank == slot, here, 0.0)
    pick = back.T[:SLOTS].astype(BF16)
    back = back.astype(BF16)

    arrived(r1.at[pl.ds(0, 31)], P1)
    for i in range(32):
        lhs[2 * i : 2 * i + 2, :] = r1[i]
    arrived(wbuf.at[pl.ds(0, 496), :], W)
    part[...] = dot(lhs[...].astype(BF16), wbuf[...])
    for i in range(32):
        s2[i] = part[2 * i : 2 * i + 2, :]

    def send_2(r, carry):
        t = (plane + r) % 32
        remote(s2.at[t], r2.at[plane], P2, z * 32 + t).start()
        return carry

    lax.fori_loop(1, 32, send_2, 0)
    r2[plane] = s2[plane]
    arrived(r2.at[pl.ds(0, 31)], P2)

    for u in range(24):
        cb, at = u // 3, (u % 3) * 128
        val = r2[cb, :, at : at + 128]
        for yy in range(1, 4):
            val = val + r2[yy * 8 + cb, :, at : at + 128]
        for s in range(2):
            line = val[s : s + 1, :]
            if u < 16:
                r = (u % 2) * 8 + u // 2
                qscr[s, r : r + 1, :] = line
            elif u < 20:
                kscr[s, u - 16 : u - 15, :] = line
            else:
                v = u - 20
                vscr[s, v // 2 : v // 2 + 1, (v % 2) * 128 : (v % 2) * 128 + 128] = line

    for c in locals_[4:6]:
        c.wait()
    rows = lax.broadcasted_iota(jnp.int32, (16, 1), 0)
    pair_of = (rows // 8) + 2 * ((rows % 8) // 4)
    head = lax.broadcasted_iota(jnp.int32, (8, 1), 0)
    diag = lax.broadcasted_iota(jnp.int32, (8, 8), 0) == lax.broadcasted_iota(jnp.int32, (8, 8), 1)
    lam_col = jnp.sum(jnp.where(diag, lam[...], 0.0), axis=1, keepdims=True)
    scale = 128 ** (-0.5)
    place = lax.broadcasted_iota(jnp.int32, (1, CACHE), 1)
    for s in range(2):
        cos_row, sin_row = cosine[s : s + 1, :], sine[s : s + 1, :]

        def turn(v):
            return (v * cos_row + pltpu.roll(v, 64, 1) * sin_row).astype(BF16)

        q = turn(qscr[s]).astype(F32)
        kn = turn(kscr[s])
        vn = vscr[s].astype(BF16)
        for u in range(4):
            key_out[s : s + 1, u * 128 : u * 128 + 128] = kn[u : u + 1]
        for u in range(2):
            val_out[s : s + 1, u * 256 : u * 256 + 256] = vn[u : u + 1]
        kn = kn.astype(F32)
        vn = vn.astype(F32)
        wide = jnp.concatenate([jnp.where(pair_of == u, q, 0.0) for u in range(4)], axis=1).astype(BF16)
        scores = lax.dot_general(wide, kc[s], (((1,), (1,)), ((), ())), preferred_element_type=F32) * scale
        k_of = jnp.where(
            pair_of == 0, kn[0:1], jnp.where(pair_of == 1, kn[1:2], jnp.where(pair_of == 2, kn[2:3], kn[3:4]))
        )
        own_score = jnp.sum(q * k_of, axis=1, keepdims=True) * scale
        live = place < lengths[s]
        peak = jnp.maximum(jnp.max(jnp.where(live, scores, -jnp.inf), axis=1, keepdims=True), own_score)
        weights = jnp.where(live, jnp.exp(scores - peak), 0.0)
        own_weight = jnp.exp(own_score - peak)
        totals = jnp.sum(weights, axis=1, keepdims=True) + own_weight
        maps = weights / totals
        own_maps = own_weight / totals
        combined = (maps[:8] - lam_col * maps[8:]).astype(BF16)
        own_comb = (own_maps[:8] - lam_col * own_maps[8:]).astype(BF16).astype(F32)
        both = dot(combined, vc[s])
        first = head < 4
        head_out = jnp.where(first, both[:, :256], both[:, 256:])
        head_out = head_out + own_comb * jnp.where(first, vn[0:1], vn[1:2])
        att = rms(head_out, hgain[...], 1e-5).astype(BF16).astype(F32)
        for yy in range(4):
            for zz in range(4):
                h, half = (4 * zz + yy) // 2, yy % 2
                s3[yy, s : s + 1, zz * 128 : zz * 128 + 128] = att[h : h + 1, half * 128 : half * 128 + 128]

    def send_3(r, carry):
        t = (plane + r) % 32
        remote(s3.at[t // 8], r3.at[plane], P3, z * 32 + t).start()
        return carry

    lax.fori_loop(1, 32, send_3, 0)
    r3[plane] = s3[y]
    arrived(obuf.at[pl.ds(0, 496), :], O)
    arrived(hbuf.at[pl.ds(0, 7)], HID)
    arrived(r3.at[pl.ds(0, 31)], P3)
    left(r1.at[pl.ds(0, 31)], P1)
    for i in range(32):
        lhs[2 * i : 2 * i + 2, :] = r3[i]
    proj = dot(lhs[...].astype(BF16), obuf[...])
    s2b = part
    s2b[:, :256] = proj

    def send_4(r, carry):
        t = (y + r) % 4
        remote(
            s2b.at[pl.ds(pl.multiple_of(t * 16, 16), 16), pl.ds(0, 256)], r4.at[y], P4, z * 32 + t * 8 + xc
        ).start()
        return carry

    lax.fori_loop(1, 4, send_4, 0)
    r4[y] = s2b[pl.ds(pl.multiple_of(y * 16, 16), 16), pl.ds(0, 256)]
    for i in range(8):
        lhs[2 * i : 2 * i + 2, 0:256] = hbuf[i]
    arrived(r4.at[pl.ds(0, 3)], P4)
    proj = (r4[0] + r4[1]) + (r4[2] + r4[3])
    mixed = (lhs[0:16, 0:256] + proj.astype(BF16).astype(F32)).astype(BF16)
    am[...] = mixed
    gat[xc, row] = mixed

    def send_5(r, carry):
        remote(am, gat.at[xc, row], P5, (me + r) % N).start()
        return carry

    lax.fori_loop(1, N, send_5, 0)
    for c in locals_[6:]:
        c.wait()
    arrived(racc.at[pl.ds(0, N - 1)], P5)

    def normed_rows(blocks):
        total = jnp.sum(blocks[0] * blocks[0], axis=1, keepdims=True)
        for b in blocks[1:]:
            total = total + jnp.sum(b * b, axis=1, keepdims=True)
        factor = lax.rsqrt(total / D + 1e-6)
        return jnp.concatenate(
            [(b * factor * mgain[:, i * 256 : i * 256 + 256]).astype(BF16) for i, b in enumerate(blocks)], axis=1
        )

    moe = normed_rows([dot(pick, gat[b].reshape(256, 256)) for b in range(8)])
    hid = (jax.nn.silu(dot(moe, gate[...])) * dot(moe, up[...])).astype(BF16)
    answer = dot(hid, down[...]).astype(BF16)
    answer = jnp.concatenate([answer, jnp.zeros((128 - SLOTS, D), BF16)], axis=0)
    for b in range(8):
        spread = dot(back, answer[:, b * 256 : b * 256 + 256]) * wcol
        res[b] = spread.astype(BF16).reshape(16, 16, 256)

    def send_6(r, carry):
        t = (me + r) % N
        remote(res.at[t % 8, t // 8], racc.at[me], P6, t).start()
        return carry

    lax.fori_loop(1, N, send_6, 0)
    racc[me] = res[xc, row]

    moe = normed_rows([gat[b, row].astype(F32) for b in range(8)])
    hid = (jax.nn.silu(dot(moe, sg[...])) * dot(moe, su[...])).astype(BF16)
    total = dot(hid, sd[...])
    arrived(racc.at[pl.ds(0, N - 1)], P6)

    def add(i, carry):
        return carry + racc[i].astype(F32)

    total = am[...].astype(F32) + (lax.fori_loop(0, N, add, jnp.zeros((16, 256), F32)) + total)
    total = total.astype(BF16).astype(F32)
    for i in range(8):
        s7[i] = total[2 * i : 2 * i + 2, :]

    def send_7(r, carry):
        t = (xc + r) % 8
        remote(s7.at[t], r7.at[xc], P7, row * 8 + t).start()
        return carry

    lax.fori_loop(1, 8, send_7, 0)
    r7[xc] = s7[xc]
    left(wbuf.at[pl.ds(0, 496), :], W)
    left(obuf.at[pl.ds(0, 496), :], O)
    left(hbuf.at[pl.ds(0, 7)], HID)
    left(r2.at[pl.ds(0, 31)], P2)
    left(r3.at[pl.ds(0, 31)], P3)
    left(r4.at[pl.ds(0, 3)], P4)
    left(racc.at[pl.ds(0, N - 1)], P5)
    left(racc.at[pl.ds(0, N - 1)], P6)
    arrived(r7.at[pl.ds(0, 7)], P7)
    for j in range(8):
        out[:, j * 256 : j * 256 + 256] = r7[j].astype(BF16)
    left(r7.at[pl.ds(0, 7)], P7)


def on_device(
    hidden_in, lengths, key_cache, value_cache, query_w, key_w, value_w, out_w, lam_heads, head_gain,
    attn_gain, moe_gain, routing, route_weight, gate_w, up_w, down_w, shared_gate, shared_up, shared_down,
):
    inverse = 500000.0 ** (-jnp.arange(64, dtype=F32) / 64)
    angles = lengths.astype(F32)[:, None] * inverse
    cosine, sine = jnp.cos(angles), jnp.sin(angles)
    cosine = jnp.concatenate([cosine, cosine], axis=1)
    sine = jnp.concatenate([-sine, sine], axis=1)
    vm = pl.BlockSpec(memory_space=pltpu.VMEM)
    hbm = pl.BlockSpec(memory_space=ANY)
    scratch = [
        ((16, 3072), BF16), ((16, 2048), BF16), ((512, 384), BF16), ((512, 256), BF16),
        ((2, CACHE, 512), BF16), ((2, CACHE, 512), BF16),
        ((D, 512), BF16), ((D, 512), BF16), ((512, D), BF16),
        ((D, 512), BF16), ((D, 512), BF16), ((512, 256), BF16),
        ((8, 2, 256), F32), ((8, 2, 256), F32), ((4, 2, 512), F32), ((32, 2, 512), F32),
        ((64, 512), F32), ((64, 384), F32), ((32, 2, 384), F32), ((32, 2, 384), F32),
        ((2, 16, 128), F32), ((2, 4, 128), F32), ((2, 2, 256), F32),
        ((4, 2, 512), F32), ((32, 2, 512), F32), ((4, 16, 256), F32), ((16, 256), BF16),
        ((8, 16, 16, 256), BF16), ((8, 16, 16, 256), BF16), ((N, 16, 256), BF16),
        ((8, 2, 256), F32), ((8, 2, 256), F32),
    ]
    return pl.pallas_call(
        kernel,
        out_shape=(
            jax.ShapeDtypeStruct((2, D), BF16),
            jax.ShapeDtypeStruct((2, 512), BF16),
            jax.ShapeDtypeStruct((2, 512), BF16),
        ),
        in_specs=[pl.BlockSpec(memory_space=pltpu.SMEM)] + [vm] * 9 + [hbm] * 12,
        out_specs=(vm, vm, vm),
        scratch_shapes=[pltpu.VMEM(*s) for s in scratch]
        + [pltpu.SemaphoreType.DMA((12,)), pltpu.SemaphoreType.DMA((10,)), pltpu.SemaphoreType.DMA((10,))],
        compiler_params=pltpu.CompilerParams(
            collective_id=0, has_side_effects=True, vmem_limit_bytes=60 * 1024 * 1024
        ),
    )(
        lengths, hidden_in, cosine, sine, lam_heads.reshape(1, 8), head_gain.reshape(1, 256),
        attn_gain.reshape(1, D), moe_gain.reshape(1, D), routing, route_weight,
        query_w, key_w, value_w, out_w, key_cache, value_cache, gate_w, up_w, down_w,
        shared_gate, shared_up, shared_down,
    )


def solution(mesh):
    e2, e3 = P("ep", None), P("ep", None, None)
    return jax.shard_map(
        on_device,
        mesh=mesh,
        in_specs=(
            e2, P("ep"), e3, e3, e2, e2, e2, e2, P(), P(), P(), P(), P(), P(), e3, e3, e3, P(), P(), P(),
        ),
        out_specs=(e2, e2, e2),
        check_vma=False,
    )
```

time: 222 us -> 85.5 us (0.39)
  waiting for transfers between devices: 107 us -> 0 us
  Pallas kernels: 0 us -> 75.3 us
  starting transfers between devices: 31.8 us -> 0 us
  blocking collectives: 18.5 us -> 0 us
  matrix products: 17.3 us -> 0 us
  local copies, waits for them, and re-layouts: 20.6 us -> 6.78 us
  between operations: 14.3 us -> 0.65 us
  other arithmetic: 11.2 us -> 1.43 us
    pallas_call x0 -> x1, Pallas kernels: none -> 75.3 us  [on_device(): pl.pallas_call(kernel, out_shape=(jax.ShapeDtypeStruct((2, D), BF16), jax...]
    all_to_all x5 -> x0, waiting for transfers between devices: 62.5 us -> none  [the longest x1 18.5 us: on_device(): lax.all_to_all(outgoing, EP, split_axis=0, concat_axis=0, tiled=True)]
    all_gather x1 -> x0, waiting for transfers between devices: 44 us -> none  [on_device(): all_rows = lax.all_gather(hidden_in, EP, axis=0, tiled=True)]
    all_to_all x5 -> x0, starting transfers between devices: 31.7 us -> none  [the longest x1 11.2 us: on_device(): lax.all_to_all(joined_rows, EP, split_axis=1, concat_axis=0, tiled=True)]
    all_to_all x2 -> x0, blocking collectives: 18.5 us -> none  [the longest x1 14 us: on_device(): lax.all_to_all(attn_out, EP, split_axis=1, concat_axis=0, tiled=True)]
    dot_general x11 -> x0, matrix products: 17.3 us -> none  [the longest x1 3.56 us: on_device(): jnp.dot(shared_hidden, shared_down, preferred_element_type=jnp.float32)]
    reduce_sum x8 -> x0, other arithmetic: 7.08 us -> none  [the longest x1 3.08 us: sent_and_summed(): return arrived.astype(jnp.float32).sum(axis=0)]
    reshape x5 -> x0, local copies, waits for them, and re-layouts: 6.75 us -> none  [the longest x1 3.98 us: attend(): cache_keys = cache_keys.reshape(num_seqs, cache_len, kv_heads, 2, head_dim)]
  transfers between devices with their start and end apart: 6 -> 0, of which waited for: 6 -> 0; matrix products, arithmetic and copies ran while one was open for 5% -> 0% of each run, Pallas kernels for 0% -> 0%
where the time goes in v1:
time: 85.5 us; the launch traced here: 84.2 us
  Pallas kernels  75.3 us (88%)
  local copies, waits for them, and re-layouts  6.78 us (8%)
  other arithmetic  1.43 us (2%)
    pallas_call x1, Pallas kernels, on_device(): pl.pallas_call(kernel, out_shape=(jax.ShapeDtypeStruct((2, D), BF16), jax...  75.3 us
    unnamed x5, local copies, waits for them, and re-layouts  6.78 us

profile of v1, /device:TPU:0, one launch (start us, length us, event | category | flops | bytes accessed | tf_op | source)
XLA Modules:
  0.0 84.2 jit_solution(14185866503698364868)
XLA Ops:
  0.6 0.7 convert_element_type.3
  1.3 0.1 fusion
  1.4 0.6 pad_maximum_fusion
  2.1 1.5 %copy.23.routing = s32[256,6]{1,0:T(8,128)} copy(s32[256,6]{0,1:T(8,128)} %param.32) | data formatting | bytes 12288 | tf_op args[12]
  3.5 1.5 %copy.24.rweight = f32[256,6]{1,0:T(8,128)} copy(f32[256,6]{0,1:T(8,128)} %param.33) | data formatting | bytes 12288 | tf_op args[13]
  5.0 75.3 %shard_map.211 = (bf16[2,2048]{1,0:T(2,128)(2,1)}, bf16[2,512]{1,0:T(2,128)(2,1)}, bf16[2,512]{1,0:T(2,128)(2,1)}) custom-call(s32[2]{0:T(128)} %lengths.1, bf16[2,2048]{1,0:T(2,128)(2,1)} %hidden.1, f32[2,128]{1,0:T(2,128)} %get-tuple-element.6.cosine, f32[2,128]{1,0:T(2,128)} %get-tuple-element.7.sine, f32[1,8]{1,0:T(1,128)} %bitcast.7, f32[1,256]{1,0:T(1,128)} %bitcast.6, ...), custom_call_target="tpu_custom_call" | custom-call | tf_op jit(solution)/shard_map/pallas_call | solution.py:350
  80.4 1.3 %copy.28 = bf16[2,2048]{1,0:T(2,128)(2,1)} copy(bf16[2,2048]{1,0:T(2,128)(2,1)} %get-tuple-element.11) | data formatting | bytes 16384
  81.7 1.3 %copy.29 = bf16[2,512]{1,0:T(2,128)(2,1)} copy(bf16[2,512]{1,0:T(2,128)(2,1)} %get-tuple-element.12) | data formatting | bytes 4096
  82.9 1.3 %copy.30 = bf16[2,512]{1,0:T(2,128)(2,1)} copy(bf16[2,512]{1,0:T(2,128)(2,1)} %get-tuple-element.13) | data formatting | bytes 4096
  (1 shorter events, 0.0 us)

commit v2 on v1

v2 whole, which is shorter than its diff:
```python
import jax
import jax.numpy as jnp
from jax import lax
from jax.experimental import pallas as pl
from jax.experimental.pallas import tpu as pltpu
from jax.sharding import PartitionSpec as P

F32 = jnp.float32
BF16 = jnp.bfloat16
MESH = pl.DeviceIdType.MESH
N = 128
CHIPS = 64
D = 2048
CACHE = 1024
SLOTS = 32
OWN = 24
W, O, OX, HID, P1, P2, P3, P5, PX, AX, P6 = range(11)


def dot(a, b):
    return jnp.dot(a, b, preferred_element_type=F32)


def dot_nt(a, b):
    return lax.dot_general(a, b, (((1,), (1,)), ((), ())), preferred_element_type=F32)


def iota(shape, dim):
    return lax.broadcasted_iota(jnp.int32, shape, dim)


def rms(x, gain, eps):
    return x * lax.rsqrt(jnp.mean(x * x, axis=-1, keepdims=True) + eps) * gain


def kernel(
    lengths_h, hidden_h, lam_h, hgain_h, again_h, mgain_h, routing_h, rweight_h,
    qw, kw, vw, ow, kc_h, vc_h, gate_h, up_h, down_h, sg_h, su_h, sd_h,
    out,
    lengths, hidden, lam, hgain, again, mgain, routing, rweight,
    wcat, obuf_s, wbuf, obuf, kc, vc, gate, up, down, sg, su, sd,
    hs, hbuf, hb, s1, r1, lhs, part, s2, r2, qscr, kscr, vscr, at16, s3, r3, x3,
    am, gat, pt8, spread, mine, theirs, picked, ans, ans_x, res, racc, fin,
    loc, snd, rcv,
):
    me = lax.axis_index("ep")
    z = me // 32
    plane = me % 32
    y = plane // 8
    xc = me % 8
    c = me % 2
    chip = me // 2
    q = chip % 16
    slab = z * 8 + xc
    mate = me + 1 - 2 * c

    barrier = pltpu.get_barrier_semaphore()

    def greet(device):
        pl.semaphore_signal(barrier, inc=1, device_id=(device,), device_id_type=MESH)

    def greet_same(r, carry):
        greet((chip + r) % CHIPS * 2 + c)
        return carry

    def greet_plane(r, carry):
        greet(z * 32 + r * 2 + 1 - c)
        return carry

    def greet_slab(r, carry):
        greet((z + r // 4) % 4 * 32 + y * 8 + (r % 4) * 2 + 1 - c)
        return carry

    lax.fori_loop(1, CHIPS, greet_same, 0)
    lax.fori_loop(0, 16, greet_plane, 0)
    lax.fori_loop(4, 16, greet_slab, 0)

    pairs = [
        (hidden_h, hidden), (again_h, again),
        (qw, wcat.at[:, pl.ds(0, 2048)]), (kw, wcat.at[:, pl.ds(2048, 512)]), (vw, wcat.at[:, pl.ds(2560, 512)]),
        (routing_h, routing), (rweight_h, rweight), (ow, obuf_s),
        (kc_h, kc), (vc_h, vc), (lengths_h, lengths), (lam_h, lam), (hgain_h, hgain), (mgain_h, mgain),
        (gate_h.at[0], gate), (up_h.at[0], up), (down_h.at[0], down), (sg_h, sg), (su_h, su), (sd_h, sd),
    ]
    copies = [pltpu.make_async_copy(src, dst, loc.at[i]) for i, (src, dst) in enumerate(pairs)]
    for copy in copies:
        copy.start()

    def ready(lo, hi):
        for copy in copies[lo:hi]:
            copy.wait()

    def remote(src, dst, phase, device):
        return pltpu.make_async_remote_copy(
            src_ref=src, dst_ref=dst, send_sem=snd.at[phase], recv_sem=rcv.at[phase],
            device_id=(device,), device_id_type=MESH,
        )

    def arrived(ref, phase):
        remote(ref, ref, phase, mate).wait_recv()

    def left(ref, phase):
        remote(ref, ref, phase, mate).wait_send()

    ready(0, 2)
    h32 = hidden[...].astype(F32)
    normed = rms(h32, again[...], 1e-6).astype(BF16).astype(F32)
    for yy in range(4):
        for zz in range(4):
            s1[yy, :, zz * 128 : zz * 128 + 128] = normed[:, zz * 512 + yy * 128 : zz * 512 + yy * 128 + 128]
    for j in range(16):
        hs[j] = h32[:, j * 128 : j * 128 + 128]
    ready(2, 5)
    pl.semaphore_wait(barrier, 91)

    def send_1(r, carry):
        t = (plane + r) % 32
        remote(s1.at[t // 8], r1.at[plane], P1, z * 32 + t).start()
        return carry

    def send_w(r, carry):
        t = (slab + r) % 32
        col = pl.multiple_of((t % 8) * 384, 128)
        at = pl.multiple_of(slab * 16, 16)
        remote(wcat.at[:, pl.ds(col, 384)], wbuf.at[pl.ds(at, 16), :], W, (t // 8) * 32 + y * 8 + t % 8).start()
        return carry

    def send_h(r, carry):
        t = (q + r) % 16
        remote(hs.at[t], hbuf.at[q], HID, z * 32 + t * 2 + c).start()
        return carry

    def send_o(r, carry):
        t = (chip + r) % CHIPS
        col = pl.multiple_of((t % 16) * 128, 128)
        remote(obuf_s.at[:, pl.ds(col, 128)], obuf.at[chip, c], O, t * 2 + c).start()
        return carry

    lax.fori_loop(1, 32, send_w, 0)
    lax.fori_loop(1, 32, send_1, 0)
    own = pl.ds(pl.multiple_of(slab * 16, 16), 16)
    wbuf[own, :] = wcat[:, pl.ds(pl.multiple_of(xc * 384, 128), 384)]
    r1[plane] = s1[y]
    hbuf[q] = hs[q]

    ready(5, 8)
    obuf[chip, c] = obuf_s[:, pl.ds(pl.multiple_of(q * 128, 128), 128)]
    sel = jnp.where(
        iota((128, 256), 1) == 4 * (iota((128, 256), 0) // 2) + 2 * c + iota((128, 256), 0) % 2, 1.0, 0.0
    ).astype(BF16)
    before = jnp.where(iota((256, 256), 0) < iota((256, 256), 1), 1.0, 0.0).astype(BF16)
    picks = []
    for i, expert in enumerate((me, mate)):
        hit = routing[...] == expert
        here = jnp.sum(jnp.where(hit, 1.0, 0.0), axis=0, keepdims=True)
        rank = dot(jnp.broadcast_to(here, (16, 256)).astype(BF16), before)[0:1]
        full = jnp.where(rank == (iota((256, 256), 0) % SLOTS).astype(F32), here, 0.0)
        pt8[i] = dot_nt(sel, full.astype(BF16))
        full = full[:SLOTS]
        if i == 0:
            weight = jnp.sum(jnp.where(hit, rweight[...], 0.0), axis=0, keepdims=True)
            weight = jnp.sum(full * weight, axis=1, keepdims=True)
        mark = (iota((SLOTS, 256), 0) - OWN == iota((SLOTS, 256), 1) - 2 * expert) & (
            iota((SLOTS, 256), 1) // 2 == expert
        )
        full = full + jnp.where(mark, 1.0, 0.0)
        picks.append(dot_nt(full.astype(BF16), sel))
    picks = jnp.concatenate(picks, axis=0).astype(BF16)
    block = (iota((16, 256), 1) // SLOTS) == (iota((16, 256), 0) % 8)
    first_token = iota((16, 256), 0) < 8

    def lay(g, carry):
        for i in range(2):
            eight = pt8[i, pl.ds(pl.multiple_of(8 * g, 8), 8), :]
            for o in range(4):
                tile = jnp.where(first_token, eight[2 * o : 2 * o + 1], eight[2 * o + 1 : 2 * o + 2])
                spread[i, 4 * g + o] = jnp.where(block, tile, 0.0).astype(BF16)
        return carry

    arrived(r1.at[pl.ds(0, 31)], P1)
    for i in range(32):
        lhs[2 * i : 2 * i + 2, :] = r1[i]
    arrived(wbuf.at[pl.ds(0, 496), :], W)
    part[...] = dot(lhs[...].astype(BF16), wbuf[...])
    for i in range(32):
        s2[i] = part[2 * i : 2 * i + 2, :]

    def send_2(r, carry):
        t = (plane + r) % 32
        remote(s2.at[t], r2.at[plane], P2, z * 32 + t).start()
        return carry

    lax.fori_loop(1, 32, send_2, 0)
    r2[plane] = s2[plane]
    lax.fori_loop(1, CHIPS, send_o, 0)
    lax.fori_loop(1, 16, send_h, 0)
    lax.fori_loop(0, CHIPS // 4, lay, 0)
    arrived(r2.at[pl.ds(0, 31)], P2)

    for u in range(24):
        cb, at = u // 3, (u % 3) * 128
        val = r2[cb, :, at : at + 128]
        for yy in range(1, 4):
            val = val + r2[yy * 8 + cb, :, at : at + 128]
        for s in range(2):
            line = val[s : s + 1, :]
            if u < 16:
                r = (u % 2) * 8 + u // 2
                qscr[s, r : r + 1, :] = line
            elif u < 20:
                kscr[s, u - 16 : u - 15, :] = line
            else:
                v = u - 20
                vscr[s, v // 2 : v // 2 + 1, (v % 2) * 128 : (v % 2) * 128 + 128] = line

    ready(8, 14)
    rows = iota((16, 1), 0)
    pair_of = (rows // 8) + 2 * ((rows % 8) // 4)
    first = iota((8, 1), 0) < 4
    lam_col = jnp.sum(jnp.where(iota((8, 8), 0) == iota((8, 8), 1), lam[...], 0.0), axis=1, keepdims=True)
    scale = 128 ** (-0.5)
    place = iota((1, CACHE), 1)
    lane = iota((1, 128), 1)
    inverse = jnp.exp((lane % 64).astype(F32) * (-13.122363377404328 / 64))
    for s in range(2):
        angle = lengths[s].astype(F32) * inverse
        cos_row = jnp.cos(angle)
        sin_row = jnp.where(lane < 64, -jnp.sin(angle), jnp.sin(angle))

        def turn(v):
            return (v * cos_row + pltpu.roll(v, 64, 1) * sin_row).astype(BF16)

        qq = turn(qscr[s]).astype(F32)
        kn = turn(kscr[s])
        vn = vscr[s].astype(BF16)
        for u in range(4):
            out[s : s + 1, D + u * 128 : D + u * 128 + 128] = kn[u : u + 1]
        for u in range(2):
            out[s : s + 1, D + 512 + u * 256 : D + 512 + u * 256 + 256] = vn[u : u + 1]
        kn = kn.astype(F32)
        vn = vn.astype(F32)
        wide = jnp.concatenate([jnp.where(pair_of == u, qq, 0.0) for u in range(4)], axis=1).astype(BF16)
        scores = dot_nt(wide, kc[s]) * scale
        k_of = jnp.where(
            pair_of == 0, kn[0:1], jnp.where(pair_of == 1, kn[1:2], jnp.where(pair_of == 2, kn[2:3], kn[3:4]))
        )
        own_score = jnp.sum(qq * k_of, axis=1, keepdims=True) * scale
        live = place < lengths[s]
        peak = jnp.maximum(jnp.max(jnp.where(live, scores, -jnp.inf), axis=1, keepdims=True), own_score)
        weights = jnp.where(live, jnp.exp(scores - peak), 0.0)
        own_weight = jnp.exp(own_score - peak)
        totals = jnp.sum(weights, axis=1, keepdims=True) + own_weight
        maps = weights / totals
        own_maps = own_weight / totals
        combined = (maps[:8] - lam_col * maps[8:]).astype(BF16)
        own_comb = (own_maps[:8] - lam_col * own_maps[8:]).astype(BF16).astype(F32)
        both = dot(combined, vc[s])
        head_out = jnp.where(first, both[:, :256], both[:, 256:])
        head_out = head_out + own_comb * jnp.where(first, vn[0:1], vn[1:2])
        att = rms(head_out, hgain[...], 1e-5)
        for h in range(8):
            for half in range(2):
                at16[s, 2 * h + half : 2 * h + half + 1, :] = att[h : h + 1, half * 128 : half * 128 + 128]
        s3[s] = at16[s].astype(BF16)

    def send_3(r, carry):
        t = (q + r) % 16
        remote(s3, r3.at[q], P3, z * 32 + t * 2 + c).start()
        return carry

    lax.fori_loop(1, 16, send_3, 0)
    r3[q] = s3[...]
    arrived(obuf.at[pl.ds(0, 63), 0], O)
    remote(obuf.at[:, c], obuf.at[:, c], OX, mate).start()
    arrived(hbuf.at[pl.ds(0, 15)], HID)
    for i in range(16):
        hb[2 * i : 2 * i + 2, :] = hbuf[i]
    arrived(obuf.at[:, 0], OX)
    arrived(r3.at[pl.ds(0, 15)], P3)
    x3[...] = r3[...].reshape(512, 128).astype(F32)
    wide = jnp.concatenate([x3[pl.ds(b, 32, stride=16), :].astype(BF16) for b in range(16)], axis=1)
    proj = dot(wide, obuf[...].reshape(D, 128))
    mixed = (hb[...] + proj.astype(BF16).astype(F32)).astype(BF16)
    am[...] = mixed
    gat[q, z] = mixed

    def send_5(r, carry):
        remote(am, gat.at[q, z], P5, (chip + r) % CHIPS * 2 + c).start()
        return carry

    lax.fori_loop(1, CHIPS, send_5, 0)
    ready(14, 20)
    arrived(racc.at[pl.ds(0, CHIPS - 1)], P5)
    for b in range(8):
        cols = jnp.concatenate([gat[2 * b].reshape(128, 128), gat[2 * b + 1].reshape(128, 128)], axis=1)
        got = dot(picks, cols)
        mine[:, b * 256 : b * 256 + 256] = got[:SLOTS]
        theirs[:, b * 256 : b * 256 + 256] = got[SLOTS:].astype(BF16)
    remote(theirs, picked, PX, mate).start()
    arrived(picked, PX)
    mixed = mine[...] + picked[...].astype(F32)
    moe = rms(mixed, mgain[...], 1e-6).astype(BF16)
    hid = (jax.nn.silu(dot(moe, gate[...])) * dot(moe, up[...])).astype(BF16)
    answer = dot(hid, down[...]).astype(BF16).astype(F32) * weight
    for b in range(8):
        ans[b * SLOTS : b * SLOTS + SLOTS, :] = answer[:, b * 256 : b * 256 + 256].astype(BF16)
    remote(ans, ans_x, AX, mate).start()
    hid = (jax.nn.silu(dot(moe, sg[...])) * dot(moe, su[...])).astype(BF16)
    shared = dot(hid[OWN:], sd[...])
    arrived(ans_x, AX)
    for k in (2, 1, 3, 0):
        zz = (z + k) % 4
        lines = pl.ds(pl.multiple_of(zz * 16, 16), 16)
        tiles = dot(spread[0, lines].reshape(256, 256), ans[...]) + dot(spread[1, lines].reshape(256, 256), ans_x[...])
        res[lines] = tiles.astype(BF16).reshape(16, 16, 256)

        def send_6(r, carry):
            t = zz * 16 + (q + r) % 16
            remote(res.at[t], racc.at[chip], P6, t * 2 + c).start()
            return carry

        lax.fori_loop(0 if k else 1, 16, send_6, 0)
    racc[chip] = res[chip]
    left(wbuf.at[pl.ds(0, 496), :], W)
    left(obuf.at[pl.ds(0, 63), 0], O)
    left(obuf.at[:, 0], OX)
    left(hbuf.at[pl.ds(0, 15)], HID)
    left(r1.at[pl.ds(0, 31)], P1)
    left(r2.at[pl.ds(0, 31)], P2)
    left(r3.at[pl.ds(0, 15)], P3)
    left(racc.at[pl.ds(0, CHIPS - 1)], P5)
    left(picked, PX)
    left(ans_x, AX)
    arrived(racc.at[pl.ds(0, CHIPS - 1)], P6)

    def add(i, carry):
        return carry + racc[i].astype(F32)

    total = lax.fori_loop(0, CHIPS, add, jnp.zeros((16, 256), F32), unroll=8)
    for s in range(2):
        for b in range(8):
            fin[s : s + 1, b * 256 : b * 256 + 256] = total[s * 8 + b : s * 8 + b + 1]
    out[:, 0:D] = (mixed[OWN : OWN + 2] + fin[...] + shared[0:2]).astype(BF16)
    left(racc.at[pl.ds(0, CHIPS - 1)], P6)


def on_device(
    hidden_in, lengths, key_cache, value_cache, query_w, key_w, value_w, out_w, lam_heads, head_gain,
    attn_gain, moe_gain, routing, route_weight, gate_w, up_w, down_w, shared_gate, shared_up, shared_down,
):
    hbm = pl.BlockSpec(memory_space=pl.ANY)
    scratch = [
        ((2, D), BF16), ((1, 8), F32), ((1, 256), F32), ((1, D), F32), ((1, D), F32),
        ((6, 256), jnp.int32), ((6, 256), F32),
        ((16, 3072), BF16), ((16, D), BF16), ((512, 384), BF16), ((CHIPS, 2, 16, 128), BF16),
        ((2, CACHE, 512), BF16), ((2, CACHE, 512), BF16),
        ((D, 512), BF16), ((D, 512), BF16), ((512, D), BF16),
        ((D, 512), BF16), ((D, 512), BF16), ((512, D), BF16),
        ((16, 2, 128), F32), ((16, 2, 128), F32), ((32, 128), F32),
        ((4, 2, 512), F32), ((32, 2, 512), F32), ((64, 512), F32), ((64, 384), F32),
        ((32, 2, 384), F32), ((32, 2, 384), F32),
        ((2, 16, 128), F32), ((2, 4, 128), F32), ((2, 2, 256), F32),
        ((2, 16, 128), F32), ((2, 16, 128), BF16), ((16, 2, 16, 128), BF16), ((512, 128), F32),
        ((32, 128), BF16), ((16, 4, 32, 128), BF16), ((2, 128, 256), F32), ((2, CHIPS, 16, 256), BF16),
        ((SLOTS, D), F32), ((SLOTS, D), BF16), ((SLOTS, D), BF16),
        ((256, 256), BF16), ((256, 256), BF16), ((CHIPS, 16, 256), BF16), ((CHIPS, 16, 256), BF16), ((2, D), F32),
    ]
    packed = pl.pallas_call(
        kernel,
        out_shape=jax.ShapeDtypeStruct((2, D + 1024), BF16),
        in_specs=[hbm] * 20,
        out_specs=pl.BlockSpec(memory_space=pltpu.VMEM),
        scratch_shapes=[pltpu.SMEM((2,), jnp.int32)]
        + [pltpu.VMEM(*s) for s in scratch]
        + [pltpu.SemaphoreType.DMA((20,)), pltpu.SemaphoreType.DMA((11,)), pltpu.SemaphoreType.DMA((11,))],
        compiler_params=pltpu.CompilerParams(
            collective_id=0, has_side_effects=True, vmem_limit_bytes=60 * 1024 * 1024
        ),
    )(
        lengths, hidden_in, lam_heads.reshape(1, 8), head_gain.reshape(1, 256),
        attn_gain.reshape(1, D), moe_gain.reshape(1, D), routing.T, route_weight.T,
        query_w, key_w, value_w, out_w, key_cache, value_cache, gate_w, up_w, down_w,
        shared_gate, shared_up, shared_down,
    )
    return packed[:, :D], packed[:, D : D + 512], packed[:, D + 512 :]


def solution(mesh):
    e2, e3 = P("ep", None), P("ep", None, None)
    return jax.shard_map(
        on_device,
        mesh=mesh,
        in_specs=(
            e2, P("ep"), e3, e3, e2, e2, e2, e2, P(), P(), P(), P(), P(), P(), e3, e3, e3, P(), P(), P(),
        ),
        out_specs=(e2, e2, e2),
        check_vma=False,
    )
```

time: 85.5 us -> 57.7 us (0.67); the launches traced: 84.2 us -> 57.4 us
  Pallas kernels: 75.3 us -> 54.2 us
  local copies, waits for them, and re-layouts: 6.78 us -> 2.58 us
  other arithmetic: 1.43 us -> 0 us
    pallas_call x1, Pallas kernels: 75.3 us -> 54.2 us  [on_device(): pl.pallas_call(kernel, out_shape=jax.ShapeDtypeStruct((2, D + 1024), BF16...]
    unnamed x5 -> x0, local copies, waits for them, and re-layouts: 6.78 us -> none
    slice x0 -> x2, local copies, waits for them, and re-layouts: none -> 2.58 us  [on_device(): return (packed[:, :D], packed[:, D:D + 512], packed[:, D + 512:])]
where the time goes in v2:
time: 57.7 us; the launch traced here: 57.4 us
  Pallas kernels  54.2 us (94%)
  local copies, waits for them, and re-layouts  2.58 us (4%)
  between operations  0.65 us (1%)
    pallas_call x1, Pallas kernels, on_device(): pl.pallas_call(kernel, out_shape=jax.ShapeDtypeStruct((2, D + 1024), BF16...  54.2 us
    slice x2, local copies, waits for them, and re-layouts, on_device(): return (packed[:, :D], packed[:, D:D + 512], packed[:, D + 512:])  2.58 us

profile of v2, /device:TPU:0, one launch (start us, length us, event | category | flops | bytes accessed | tf_op | source)
XLA Modules:
  0.0 57.4 jit_solution(15556839339013644080)
XLA Ops:
  0.6 54.2 %shard_map.211 = bf16[2,3072]{1,0:T(2,128)(2,1)} custom-call(s32[2]{0:T(128)} %lengths_h.1, bf16[2,2048]{1,0:T(2,128)(2,1)} %hidden_h.1, f32[1,8]{1,0:T(1,128)} %bitcast.11, f32[1,256]{1,0:T(1,128)} %bitcast.10, f32[1,2048]{1,0:T(1,128)} %bitcast.6, f32[1,2048]{1,0:T(1,128)} %bitcast.7, s32[6,256]{1,0:T(8,128)} %bitcast.8, f32[6,256]{1,0:T(8,128)} %bitcast.9, ...), custom_call_target="tpu_custom_call" | custom-call | tf_op jit(solution)/shard_map/pallas_call | solution.py:368
  54.9 1.3 %fusion = (bf16[2,512]{1,0:T(2,128)(2,1)}, bf16[2,512]{1,0:T(2,128)(2,1)}) fusion(bf16[2,3072]{1,0:T(2,128)(2,1)} %shard_map.211), kind=kLoop, calls=%fused_computation | loop fusion | bytes 8192 | tf_op jit(solution)/shard_map/slice | solution.py:385
  56.1 1.3 %slice.9 = bf16[2,2048]{1,0:T(2,128)(2,1)} slice(bf16[2,3072]{1,0:T(2,128)(2,1)} %shard_map.211), slice={[0:2], [0:2048]} | slice | bytes 16384 | tf_op jit(solution)/shard_map/slice | solution.py:385

commit v3 on v2

--- a/solution.py
+++ b/solution.py
@@ -25,6 +25,22 @@
     return lax.dot_general(a, b, (((1,), (1,)), ((), ())), preferred_element_type=F32)
 
 
+def rem(a, b):
+    return lax.rem(a, jnp.int32(b))
+
+
+def div(a, b):
+    return lax.div(a, jnp.int32(b))
+
+
+def far(pair):
+    return -sum(min(k, 4 - k) for k in pair)
+
+
+NEAR = sorted(((a, b) for a in range(4) for b in range(4)), key=far)
+ALL = sorted(((a, b, k) for a in range(4) for b in range(4) for k in range(4)), key=far)[:-1]
+
+
 def iota(shape, dim):
     return lax.broadcasted_iota(jnp.int32, shape, dim)
 
@@ -39,41 +55,41 @@
     out,
     lengths, hidden, lam, hgain, again, mgain, routing, rweight,
     wcat, obuf_s, wbuf, obuf, kc, vc, gate, up, down, sg, su, sd,
-    hs, hbuf, hb, s1, r1, lhs, part, s2, r2, qscr, kscr, vscr, at16, s3, r3, x3,
+    hs, hbuf, hb, s1f, s1, r1, x1, part, s2, r2, qscr, kscr, vscr, at16, s3, r3, x3,
     am, gat, pt8, spread, mine, theirs, picked, ans, ans_x, res, racc, fin,
-    loc, snd, rcv,
+    loc, snd, rcv, met,
 ):
     me = lax.axis_index("ep")
-    z = me // 32
-    plane = me % 32
-    y = plane // 8
-    xc = me % 8
-    c = me % 2
-    chip = me // 2
-    q = chip % 16
+    z = div(me, 32)
+    plane = rem(me, 32)
+    y = div(plane, 8)
+    xc = rem(me, 8)
+    c = rem(me, 2)
+    chip = div(me, 2)
+    q = rem(chip, 16)
     slab = z * 8 + xc
     mate = me + 1 - 2 * c
 
+    x = div(xc, 2)
+    z_at = [rem(z + k, 4) for k in range(4)]
+    y_at = [rem(y + k, 4) for k in range(4)]
+    x_at = [rem(x + k, 4) for k in range(4)]
+    plane_peers = [(dy, dx, cc) for dy, dx in NEAR for cc in (c, 1 - c)][:-2] + [(0, 0, 1 - c)]
+    plane_peers = [y_at[dy] * 8 + x_at[dx] * 2 + cc for dy, dx, cc in plane_peers]
+    slab_peers = [(dz, dx, cc) for dz, dx in NEAR for cc in (c, 1 - c)][:-2] + [(0, 0, 1 - c)]
+    far_peers = [(z_at[dz], x_at[dx] * 2 + cc) for dz, dx, cc in slab_peers if dz]
+    slab_peers = [(z_at[dz], x_at[dx] * 2 + cc) for dz, dx, cc in slab_peers]
+    chips = [z_at[dz] * 16 + y_at[dy] * 4 + x_at[dx] for dz, dy, dx in ALL]
+
     barrier = pltpu.get_barrier_semaphore()
 
-    def greet(device):
-        pl.semaphore_signal(barrier, inc=1, device_id=(device,), device_id_type=MESH)
-
-    def greet_same(r, carry):
-        greet((chip + r) % CHIPS * 2 + c)
-        return carry
-
-    def greet_plane(r, carry):
-        greet(z * 32 + r * 2 + 1 - c)
-        return carry
-
-    def greet_slab(r, carry):
-        greet((z + r // 4) % 4 * 32 + y * 8 + (r % 4) * 2 + 1 - c)
-        return carry
-
-    lax.fori_loop(1, CHIPS, greet_same, 0)
-    lax.fori_loop(0, 16, greet_plane, 0)
-    lax.fori_loop(4, 16, greet_slab, 0)
+    def greet(semaphore, device):
+        pl.semaphore_signal(semaphore, inc=1, device_id=(device,), device_id_type=MESH)
+
+    for zt, xt in far_peers:
+        greet(barrier, zt * 32 + y * 8 + xt)
+    for t in plane_peers:
+        greet(barrier, z * 32 + t)
 
     pairs = [
         (hidden_h, hidden), (again_h, again),
@@ -107,37 +123,23 @@
     normed = rms(h32, again[...], 1e-6).astype(BF16).astype(F32)
     for yy in range(4):
         for zz in range(4):
-            s1[yy, :, zz * 128 : zz * 128 + 128] = normed[:, zz * 512 + yy * 128 : zz * 512 + yy * 128 + 128]
+            for i in range(2):
+                at = zz * 512 + yy * 128
+                s1f[yy, i * 4 + zz : i * 4 + zz + 1, :] = normed[i : i + 1, at : at + 128]
+    s1[...] = s1f[...].astype(BF16)
     for j in range(16):
         hs[j] = h32[:, j * 128 : j * 128 + 128]
     ready(2, 5)
-    pl.semaphore_wait(barrier, 91)
-
-    def send_1(r, carry):
-        t = (plane + r) % 32
-        remote(s1.at[t // 8], r1.at[plane], P1, z * 32 + t).start()
-        return carry
-
-    def send_w(r, carry):
-        t = (slab + r) % 32
-        col = pl.multiple_of((t % 8) * 384, 128)
-        at = pl.multiple_of(slab * 16, 16)
-        remote(wcat.at[:, pl.ds(col, 384)], wbuf.at[pl.ds(at, 16), :], W, (t // 8) * 32 + y * 8 + t % 8).start()
-        return carry
-
-    def send_h(r, carry):
-        t = (q + r) % 16
-        remote(hs.at[t], hbuf.at[q], HID, z * 32 + t * 2 + c).start()
-        return carry
-
-    def send_o(r, carry):
-        t = (chip + r) % CHIPS
-        col = pl.multiple_of((t % 16) * 128, 128)
-        remote(obuf_s.at[:, pl.ds(col, 128)], obuf.at[chip, c], O, t * 2 + c).start()
-        return carry
-
-    lax.fori_loop(1, 32, send_w, 0)
-    lax.fori_loop(1, 32, send_1, 0)
+    pl.semaphore_wait(barrier, 55)
+
+    at = pl.multiple_of(slab * 16, 16)
+    for zt, xt in slab_peers:
+        col = pl.multiple_of(xt * 384, 128)
+        remote(wcat.at[:, pl.ds(col, 384)], wbuf.at[pl.ds(at, 16), :], W, zt * 32 + y * 8 + xt).start()
+    for t in plane_peers:
+        remote(s1.at[div(t, 8)], r1.at[plane], P1, z * 32 + t).start()
+    for t in plane_peers:
+        greet(met, z * 32 + t)
     own = pl.ds(pl.multiple_of(slab * 16, 16), 16)
     wbuf[own, :] = wcat[:, pl.ds(pl.multiple_of(xc * 384, 128), 384)]
     r1[plane] = s1[y]
@@ -178,22 +180,23 @@
         return carry
 
     arrived(r1.at[pl.ds(0, 31)], P1)
-    for i in range(32):
-        lhs[2 * i : 2 * i + 2, :] = r1[i]
+    x1[...] = r1[...].astype(F32).reshape(256, 128)
+    wide = jnp.concatenate([x1[pl.ds(b, 64, stride=4), :].astype(BF16) for b in range(4)], axis=1)
     arrived(wbuf.at[pl.ds(0, 496), :], W)
-    part[...] = dot(lhs[...].astype(BF16), wbuf[...])
+    part[...] = dot(wide, wbuf[...])
     for i in range(32):
         s2[i] = part[2 * i : 2 * i + 2, :]
 
-    def send_2(r, carry):
-        t = (plane + r) % 32
+    for t in plane_peers:
         remote(s2.at[t], r2.at[plane], P2, z * 32 + t).start()
-        return carry
-
-    lax.fori_loop(1, 32, send_2, 0)
     r2[plane] = s2[plane]
-    lax.fori_loop(1, CHIPS, send_o, 0)
-    lax.fori_loop(1, 16, send_h, 0)
+    pl.semaphore_wait(met, 31)
+    for t in chips:
+        col = pl.multiple_of(rem(t, 16) * 128, 128)
+        remote(obuf_s.at[:, pl.ds(col, 128)], obuf.at[chip, c], O, t * 2 + c).start()
+    for dy, dx in NEAR[:-1]:
+        t = y_at[dy] * 4 + x_at[dx]
+        remote(hs.at[t], hbuf.at[q], HID, z * 32 + t * 2 + c).start()
     lax.fori_loop(0, CHIPS // 4, lay, 0)
     arrived(r2.at[pl.ds(0, 31)], P2)
 
@@ -250,8 +253,9 @@
         weights = jnp.where(live, jnp.exp(scores - peak), 0.0)
         own_weight = jnp.exp(own_score - peak)
         totals = jnp.sum(weights, axis=1, keepdims=True) + own_weight
-        maps = weights / totals
-        own_maps = own_weight / totals
+        share = 1.0 / totals
+        maps = weights * share
+        own_maps = own_weight * share
         combined = (maps[:8] - lam_col * maps[8:]).astype(BF16)
         own_comb = (own_maps[:8] - lam_col * own_maps[8:]).astype(BF16).astype(F32)
         both = dot(combined, vc[s])
@@ -263,12 +267,9 @@
                 at16[s, 2 * h + half : 2 * h + half + 1, :] = att[h : h + 1, half * 128 : half * 128 + 128]
         s3[s] = at16[s].astype(BF16)
 
-    def send_3(r, carry):
-        t = (q + r) % 16
+    for dy, dx in NEAR[:-1]:
+        t = y_at[dy] * 4 + x_at[dx]
         remote(s3, r3.at[q], P3, z * 32 + t * 2 + c).start()
-        return carry
-
-    lax.fori_loop(1, 16, send_3, 0)
     r3[q] = s3[...]
     arrived(obuf.at[pl.ds(0, 63), 0], O)
     remote(obuf.at[:, c], obuf.at[:, c], OX, mate).start()
@@ -284,11 +285,8 @@
     am[...] = mixed
     gat[q, z] = mixed
 
-    def send_5(r, carry):
-        remote(am, gat.at[q, z], P5, (chip + r) % CHIPS * 2 + c).start()
-        return carry
-
-    lax.fori_loop(1, CHIPS, send_5, 0)
+    for t in chips:
+        remote(am, gat.at[q, z], P5, t * 2 + c).start()
     ready(14, 20)
     arrived(racc.at[pl.ds(0, CHIPS - 1)], P5)
     for b in range(8):
@@ -305,22 +303,17 @@
     for b in range(8):
         ans[b * SLOTS : b * SLOTS + SLOTS, :] = answer[:, b * 256 : b * 256 + 256].astype(BF16)
     remote(ans, ans_x, AX, mate).start()
+    arrived(ans_x, AX)
+    for k in (2, 1, 3, 0):
+        lines = pl.ds(pl.multiple_of(z_at[k] * 16, 16), 16)
+        tiles = dot(spread[0, lines].reshape(256, 256), ans[...]) + dot(spread[1, lines].reshape(256, 256), ans_x[...])
+        res[lines] = tiles.astype(BF16).reshape(16, 16, 256)
+        for dy, dx in NEAR if k else NEAR[:-1]:
+            t = z_at[k] * 16 + y_at[dy] * 4 + x_at[dx]
+            remote(res.at[t], racc.at[chip], P6, t * 2 + c).start()
+    racc[chip] = res[chip]
     hid = (jax.nn.silu(dot(moe, sg[...])) * dot(moe, su[...])).astype(BF16)
     shared = dot(hid[OWN:], sd[...])
-    arrived(ans_x, AX)
-    for k in (2, 1, 3, 0):
-        zz = (z + k) % 4
-        lines = pl.ds(pl.multiple_of(zz * 16, 16), 16)
-        tiles = dot(spread[0, lines].reshape(256, 256), ans[...]) + dot(spread[1, lines].reshape(256, 256), ans_x[...])
-        res[lines] = tiles.astype(BF16).reshape(16, 16, 256)
-
-        def send_6(r, carry):
-            t = zz * 16 + (q + r) % 16
-            remote(res.at[t], racc.at[chip], P6, t * 2 + c).start()
-            return carry
-
-        lax.fori_loop(0 if k else 1, 16, send_6, 0)
-    racc[chip] = res[chip]
     left(wbuf.at[pl.ds(0, 496), :], W)
     left(obuf.at[pl.ds(0, 63), 0], O)
     left(obuf.at[:, 0], OX)
@@ -357,7 +350,7 @@
         ((D, 512), BF16), ((D, 512), BF16), ((512, D), BF16),
         ((D, 512), BF16), ((D, 512), BF16), ((512, D), BF16),
         ((16, 2, 128), F32), ((16, 2, 128), F32), ((32, 128), F32),
-        ((4, 2, 512), F32), ((32, 2, 512), F32), ((64, 512), F32), ((64, 384), F32),
+        ((4, 8, 128), F32), ((4, 8, 128), BF16), ((32, 8, 128), BF16), ((256, 128), F32), ((64, 384), F32),
         ((32, 2, 384), F32), ((32, 2, 384), F32),
         ((2, 16, 128), F32), ((2, 4, 128), F32), ((2, 2, 256), F32),
         ((2, 16, 128), F32), ((2, 16, 128), BF16), ((16, 2, 16, 128), BF16), ((512, 128), F32),
@@ -372,7 +365,8 @@
         out_specs=pl.BlockSpec(memory_space=pltpu.VMEM),
         scratch_shapes=[pltpu.SMEM((2,), jnp.int32)]
         + [pltpu.VMEM(*s) for s in scratch]
-        + [pltpu.SemaphoreType.DMA((20,)), pltpu.SemaphoreType.DMA((11,)), pltpu.SemaphoreType.DMA((11,))],
+        + [pltpu.SemaphoreType.DMA((20,)), pltpu.SemaphoreType.DMA((11,)), pltpu.SemaphoreType.DMA((11,))]
+        + [pltpu.SemaphoreType.REGULAR],
         compiler_params=pltpu.CompilerParams(
             collective_id=0, has_side_effects=True, vmem_limit_bytes=60 * 1024 * 1024
         ),

time: 57.7 us -> 54 us (0.936)
  Pallas kernels: 54.2 us -> 50.6 us
    pallas_call x1, Pallas kernels: 54.2 us -> 50.6 us  [on_device(): pl.pallas_call(kernel, out_shape=jax.ShapeDtypeStruct((2, D + 1024), BF16...]
where the time goes in v3:
time: 54 us; the launch traced here: 53.8 us
  Pallas kernels  50.6 us (94%)
  local copies, waits for them, and re-layouts  2.58 us (5%)
  between operations  0.65 us (1%)
    pallas_call x1, Pallas kernels, on_device(): pl.pallas_call(kernel, out_shape=jax.ShapeDtypeStruct((2, D + 1024), BF16...  50.6 us
    slice x2, local copies, waits for them, and re-layouts, on_device(): return (packed[:, :D], packed[:, D:D + 512], packed[:, D + 512:])  2.58 us

profile of v3, /device:TPU:0, one launch (start us, length us, event | category | flops | bytes accessed | tf_op | source)
XLA Modules:
  0.0 53.8 jit_solution(17411874452192495499)
XLA Ops:
  0.6 50.6 %shard_map.211 = bf16[2,3072]{1,0:T(2,128)(2,1)} custom-call(s32[2]{0:T(128)} %lengths_h.1, bf16[2,2048]{1,0:T(2,128)(2,1)} %hidden_h.1, f32[1,8]{1,0:T(1,128)} %bitcast.11, f32[1,256]{1,0:T(1,128)} %bitcast.10, f32[1,2048]{1,0:T(1,128)} %bitcast.6, f32[1,2048]{1,0:T(1,128)} %bitcast.7, s32[6,256]{1,0:T(8,128)} %bitcast.8, f32[6,256]{1,0:T(8,128)} %bitcast.9, ...), custom_call_target="tpu_custom_call" | custom-call | tf_op jit(solution)/shard_map/pallas_call | solution.py:361
  51.2 1.3 %fusion = (bf16[2,512]{1,0:T(2,128)(2,1)}, bf16[2,512]{1,0:T(2,128)(2,1)}) fusion(bf16[2,3072]{1,0:T(2,128)(2,1)} %shard_map.211), kind=kLoop, calls=%fused_computation | loop fusion | bytes 8192 | tf_op jit(solution)/shard_map/slice | solution.py:379
  52.5 1.3 %slice.9 = bf16[2,2048]{1,0:T(2,128)(2,1)} slice(bf16[2,3072]{1,0:T(2,128)(2,1)} %shard_map.211), slice={[0:2], [0:2048]} | slice | bytes 16384 | tf_op jit(solution)/shard_map/slice | solution.py:379

commit v4 on v3

--- a/solution.py
+++ b/solution.py
@@ -56,7 +56,7 @@
     lengths, hidden, lam, hgain, again, mgain, routing, rweight,
     wcat, obuf_s, wbuf, obuf, kc, vc, gate, up, down, sg, su, sd,
     hs, hbuf, hb, s1f, s1, r1, x1, part, s2, r2, qscr, kscr, vscr, at16, s3, r3, x3,
-    am, gat, pt8, spread, mine, theirs, picked, ans, ans_x, res, racc, fin,
+    am, gat, spread, mine, theirs, picked, ans, res, racc, fin,
     loc, snd, rcv, met,
 ):
     me = lax.axis_index("ep")
@@ -151,14 +151,13 @@
         iota((128, 256), 1) == 4 * (iota((128, 256), 0) // 2) + 2 * c + iota((128, 256), 0) % 2, 1.0, 0.0
     ).astype(BF16)
     before = jnp.where(iota((256, 256), 0) < iota((256, 256), 1), 1.0, 0.0).astype(BF16)
-    picks = []
+    picks, back = [], []
     for i, expert in enumerate((me, mate)):
         hit = routing[...] == expert
         here = jnp.sum(jnp.where(hit, 1.0, 0.0), axis=0, keepdims=True)
         rank = dot(jnp.broadcast_to(here, (16, 256)).astype(BF16), before)[0:1]
-        full = jnp.where(rank == (iota((256, 256), 0) % SLOTS).astype(F32), here, 0.0)
-        pt8[i] = dot_nt(sel, full.astype(BF16))
-        full = full[:SLOTS]
+        full = jnp.where(rank == iota((SLOTS, 256), 0).astype(F32), here, 0.0)
+        back.append(dot_nt(sel, full.astype(BF16)))
         if i == 0:
             weight = jnp.sum(jnp.where(hit, rweight[...], 0.0), axis=0, keepdims=True)
             weight = jnp.sum(full * weight, axis=1, keepdims=True)
@@ -168,16 +167,7 @@
         full = full + jnp.where(mark, 1.0, 0.0)
         picks.append(dot_nt(full.astype(BF16), sel))
     picks = jnp.concatenate(picks, axis=0).astype(BF16)
-    block = (iota((16, 256), 1) // SLOTS) == (iota((16, 256), 0) % 8)
-    first_token = iota((16, 256), 0) < 8
-
-    def lay(g, carry):
-        for i in range(2):
-            eight = pt8[i, pl.ds(pl.multiple_of(8 * g, 8), 8), :]
-            for o in range(4):
-                tile = jnp.where(first_token, eight[2 * o : 2 * o + 1], eight[2 * o + 1 : 2 * o + 2])
-                spread[i, 4 * g + o] = jnp.where(block, tile, 0.0).astype(BF16)
-        return carry
+    back = jnp.concatenate(back, axis=1).astype(BF16)
 
     arrived(r1.at[pl.ds(0, 31)], P1)
     x1[...] = r1[...].astype(F32).reshape(256, 128)
@@ -197,7 +187,6 @@
     for dy, dx in NEAR[:-1]:
         t = y_at[dy] * 4 + x_at[dx]
         remote(hs.at[t], hbuf.at[q], HID, z * 32 + t * 2 + c).start()
-    lax.fori_loop(0, CHIPS // 4, lay, 0)
     arrived(r2.at[pl.ds(0, 31)], P2)
 
     for u in range(24):
@@ -225,25 +214,32 @@
     place = iota((1, CACHE), 1)
     lane = iota((1, 128), 1)
     inverse = jnp.exp((lane % 64).astype(F32) * (-13.122363377404328 / 64))
+
+    def turn(v, cos_row, sin_row):
+        return (v * cos_row + pltpu.roll(v, 64, 1) * sin_row).astype(BF16)
+
+    q_rows, k_rows, v_rows, all_scores = [], [], [], []
     for s in range(2):
         angle = lengths[s].astype(F32) * inverse
         cos_row = jnp.cos(angle)
-        sin_row = jnp.where(lane < 64, -jnp.sin(angle), jnp.sin(angle))
-
-        def turn(v):
-            return (v * cos_row + pltpu.roll(v, 64, 1) * sin_row).astype(BF16)
-
-        qq = turn(qscr[s]).astype(F32)
-        kn = turn(kscr[s])
+        sin_row = jnp.sin(angle)
+        sin_row = jnp.where(lane < 64, -sin_row, sin_row)
+        qq = turn(qscr[s], cos_row, sin_row).astype(F32)
+        wide = jnp.concatenate([jnp.where(pair_of == u, qq, 0.0) for u in range(4)], axis=1).astype(BF16)
+        all_scores.append(dot_nt(wide, kc[s]))
+        kn = turn(kscr[s], cos_row, sin_row)
         vn = vscr[s].astype(BF16)
         for u in range(4):
             out[s : s + 1, D + u * 128 : D + u * 128 + 128] = kn[u : u + 1]
         for u in range(2):
             out[s : s + 1, D + 512 + u * 256 : D + 512 + u * 256 + 256] = vn[u : u + 1]
-        kn = kn.astype(F32)
-        vn = vn.astype(F32)
-        wide = jnp.concatenate([jnp.where(pair_of == u, qq, 0.0) for u in range(4)], axis=1).astype(BF16)
-        scores = dot_nt(wide, kc[s]) * scale
+        q_rows.append(qq)
+        k_rows.append(kn.astype(F32))
+        v_rows.append(vn.astype(F32))
+    sums, own_parts = [], []
+    for s in range(2):
+        qq, kn = q_rows[s], k_rows[s]
+        scores = all_scores[s] * scale
         k_of = jnp.where(
             pair_of == 0, kn[0:1], jnp.where(pair_of == 1, kn[1:2], jnp.where(pair_of == 2, kn[2:3], kn[3:4]))
         )
@@ -252,15 +248,15 @@
         peak = jnp.maximum(jnp.max(jnp.where(live, scores, -jnp.inf), axis=1, keepdims=True), own_score)
         weights = jnp.where(live, jnp.exp(scores - peak), 0.0)
         own_weight = jnp.exp(own_score - peak)
-        totals = jnp.sum(weights, axis=1, keepdims=True) + own_weight
-        share = 1.0 / totals
+        share = 1.0 / (jnp.sum(weights, axis=1, keepdims=True) + own_weight)
         maps = weights * share
         own_maps = own_weight * share
         combined = (maps[:8] - lam_col * maps[8:]).astype(BF16)
-        own_comb = (own_maps[:8] - lam_col * own_maps[8:]).astype(BF16).astype(F32)
-        both = dot(combined, vc[s])
-        head_out = jnp.where(first, both[:, :256], both[:, 256:])
-        head_out = head_out + own_comb * jnp.where(first, vn[0:1], vn[1:2])
+        own_parts.append((own_maps[:8] - lam_col * own_maps[8:]).astype(BF16).astype(F32))
+        sums.append(dot(combined, vc[s]))
+    for s in range(2):
+        head_out = jnp.where(first, sums[s][:, :256], sums[s][:, 256:])
+        head_out = head_out + own_parts[s] * jnp.where(first, v_rows[s][0:1], v_rows[s][1:2])
         att = rms(head_out, hgain[...], 1e-5)
         for h in range(8):
             for half in range(2):
@@ -301,12 +297,17 @@
     hid = (jax.nn.silu(dot(moe, gate[...])) * dot(moe, up[...])).astype(BF16)
     answer = dot(hid, down[...]).astype(BF16).astype(F32) * weight
     for b in range(8):
-        ans[b * SLOTS : b * SLOTS + SLOTS, :] = answer[:, b * 256 : b * 256 + 256].astype(BF16)
-    remote(ans, ans_x, AX, mate).start()
-    arrived(ans_x, AX)
+        ans[b, 0:SLOTS] = answer[:, b * 256 : b * 256 + 256].astype(BF16)
+    remote(ans.at[:, pl.ds(0, SLOTS)], ans.at[:, pl.ds(SLOTS, SLOTS)], AX, mate).start()
+    arrived(ans.at[:, pl.ds(0, SLOTS)], AX)
+    for b in range(8):
+        tiles = dot(back, ans[b])
+        for half in range(2):
+            spread[half, pl.ds(b, 128, stride=8), :] = tiles[:, half * 128 : half * 128 + 128]
     for k in (2, 1, 3, 0):
         lines = pl.ds(pl.multiple_of(z_at[k] * 16, 16), 16)
-        tiles = dot(spread[0, lines].reshape(256, 256), ans[...]) + dot(spread[1, lines].reshape(256, 256), ans_x[...])
+        rows = pl.ds(pl.multiple_of(z_at[k] * 256, 256), 256)
+        tiles = jnp.concatenate([spread[0, rows, :], spread[1, rows, :]], axis=1)
         res[lines] = tiles.astype(BF16).reshape(16, 16, 256)
         for dy, dx in NEAR if k else NEAR[:-1]:
             t = z_at[k] * 16 + y_at[dy] * 4 + x_at[dx]
@@ -323,7 +324,7 @@
     left(r3.at[pl.ds(0, 15)], P3)
     left(racc.at[pl.ds(0, CHIPS - 1)], P5)
     left(picked, PX)
-    left(ans_x, AX)
+    left(ans.at[:, pl.ds(0, SLOTS)], AX)
     arrived(racc.at[pl.ds(0, CHIPS - 1)], P6)
 
     def add(i, carry):
@@ -354,9 +355,9 @@
         ((32, 2, 384), F32), ((32, 2, 384), F32),
         ((2, 16, 128), F32), ((2, 4, 128), F32), ((2, 2, 256), F32),
         ((2, 16, 128), F32), ((2, 16, 128), BF16), ((16, 2, 16, 128), BF16), ((512, 128), F32),
-        ((32, 128), BF16), ((16, 4, 32, 128), BF16), ((2, 128, 256), F32), ((2, CHIPS, 16, 256), BF16),
+        ((32, 128), BF16), ((16, 4, 32, 128), BF16), ((2, 1024, 128), F32),
         ((SLOTS, D), F32), ((SLOTS, D), BF16), ((SLOTS, D), BF16),
-        ((256, 256), BF16), ((256, 256), BF16), ((CHIPS, 16, 256), BF16), ((CHIPS, 16, 256), BF16), ((2, D), F32),
+        ((8, 2 * SLOTS, 256), BF16), ((CHIPS, 16, 256), BF16), ((CHIPS, 16, 256), BF16), ((2, D), F32),
     ]
     packed = pl.pallas_call(
         kernel,
@@ -376,7 +377,24 @@
         query_w, key_w, value_w, out_w, key_cache, value_cache, gate_w, up_w, down_w,
         shared_gate, shared_up, shared_down,
     )
-    return packed[:, :D], packed[:, D : D + 512], packed[:, D + 512 :]
+
+    def unpack(src, layer, key, value):
+        layer[...] = src[:, 0:D]
+        key[...] = src[:, D : D + 512]
+        value[...] = src[:, D + 512 :]
+
+    vmem = pl.BlockSpec(memory_space=pltpu.VMEM)
+    return pl.pallas_call(
+        unpack,
+        out_shape=(
+            jax.ShapeDtypeStruct((2, D), BF16),
+            jax.ShapeDtypeStruct((2, 512), BF16),
+            jax.ShapeDtypeStruct((2, 512), BF16),
+        ),
+        in_specs=[vmem],
+        out_specs=(vmem, vmem, vmem),
+        compiler_params=pltpu.CompilerParams(vmem_limit_bytes=60 * 1024 * 1024),
+    )(packed)
 
 
 def solution(mesh):

time: 54 us -> 52.4 us (0.970)
  local copies, waits for them, and re-layouts: 2.58 us -> 0 us
  Pallas kernels: 50.6 us -> 51.5 us
    slice x2 -> x0, local copies, waits for them, and re-layouts: 2.58 us -> none  [on_device(): return (packed[:, :D], packed[:, D:D + 512], packed[:, D + 512:])]
    pallas_call x0 -> x1, Pallas kernels: none -> 1.31 us  [on_device(): pl.pallas_call(unpack, out_shape=(jax.ShapeDtypeStruct((2, D), BF16), jax...]
where the time goes in v4:
time: 52.4 us; the launch traced here: 52.1 us
  Pallas kernels  51.5 us (98%)
  between operations  0.65 us (1%)
    pallas_call x1, Pallas kernels, on_device(): pl.pallas_call(kernel, out_shape=jax.ShapeDtypeStruct((2, D + 1024), BF16...  50.2 us
    pallas_call x1, Pallas kernels, on_device(): pl.pallas_call(unpack, out_shape=(jax.ShapeDtypeStruct((2, D), BF16), jax...  1.31 us

profile of v4, /device:TPU:0, one launch (start us, length us, event | category | flops | bytes accessed | tf_op | source)
XLA Modules:
  0.0 52.1 jit_solution(17606192902156905338)
XLA Ops:
  0.6 50.2 %shard_map.211.src = bf16[2,3072]{1,0:T(2,128)(2,1)} custom-call(s32[2]{0:T(128)} %lengths_h.1, bf16[2,2048]{1,0:T(2,128)(2,1)} %hidden_h.1, f32[1,8]{1,0:T(1,128)} %bitcast.11, f32[1,256]{1,0:T(1,128)} %bitcast.10, f32[1,2048]{1,0:T(1,128)} %bitcast.6, f32[1,2048]{1,0:T(1,128)} %bitcast.7, s32[6,256]{1,0:T(8,128)} %bitcast.8, f32[6,256]{1,0:T(8,128)} %bitcast.9, ...), custom_call_target="tpu_custom_call" | custom-call | tf_op jit(solution)/shard_map/pallas_call | solution.py:362
  50.8 1.3 %shard_map.212 = (bf16[2,2048]{1,0:T(2,128)(2,1)}, bf16[2,512]{1,0:T(2,128)(2,1)}, bf16[2,512]{1,0:T(2,128)(2,1)}) custom-call(bf16[2,3072]{1,0:T(2,128)(2,1)} %shard_map.211.src), custom_call_target="tpu_custom_call" | custom-call | tf_op jit(solution)/shard_map/pallas_call | solution.py:387

commit v5 on v4

--- a/solution.py
+++ b/solution.py
@@ -14,7 +14,7 @@
 CACHE = 1024
 SLOTS = 32
 OWN = 24
-W, O, OX, HID, P1, P2, P3, P5, PX, AX, P6 = range(11)
+W, O, OX, HID, P1, P2, P3, P5, GX, UX, DX, P6 = range(12)
 
 
 def dot(a, b):
@@ -31,6 +31,10 @@
 
 def div(a, b):
     return lax.div(a, jnp.int32(b))
+
+
+def kind(v):
+    return rem(div(v + 1, 2), 2)
 
 
 def far(pair):
@@ -54,42 +58,62 @@
     qw, kw, vw, ow, kc_h, vc_h, gate_h, up_h, down_h, sg_h, su_h, sd_h,
     out,
     lengths, hidden, lam, hgain, again, mgain, routing, rweight,
-    wcat, obuf_s, wbuf, obuf, kc, vc, gate, up, down, sg, su, sd,
-    hs, hbuf, hb, s1f, s1, r1, x1, part, s2, r2, qscr, kscr, vscr, at16, s3, r3, x3,
-    am, gat, spread, mine, theirs, picked, ans, res, racc, fin,
+    wcat, obuf_s, wbuf, obuf, kc, vc, gate, up, down, gate_x, up_x, down_x, sg, su, sd,
+    hs, hbuf, hb, lines, s1f, s1, r1, x1, part, s2, r2, qscr, kscr, vscr, at16, s3, r3, x3,
+    am, gat, spread, mine, ans, res, racc, fin,
     loc, snd, rcv, met,
 ):
     me = lax.axis_index("ep")
     z = div(me, 32)
-    plane = rem(me, 32)
-    y = div(plane, 8)
+    y = rem(div(me, 8), 4)
     xc = rem(me, 8)
     c = rem(me, 2)
     chip = div(me, 2)
     q = rem(chip, 16)
-    slab = z * 8 + xc
     mate = me + 1 - 2 * c
 
     x = div(xc, 2)
     z_at = [rem(z + k, 4) for k in range(4)]
     y_at = [rem(y + k, 4) for k in range(4)]
     x_at = [rem(x + k, 4) for k in range(4)]
-    plane_peers = [(dy, dx, cc) for dy, dx in NEAR for cc in (c, 1 - c)][:-2] + [(0, 0, 1 - c)]
-    plane_peers = [y_at[dy] * 8 + x_at[dx] * 2 + cc for dy, dx, cc in plane_peers]
-    slab_peers = [(dz, dx, cc) for dz, dx in NEAR for cc in (c, 1 - c)][:-2] + [(0, 0, 1 - c)]
-    far_peers = [(z_at[dz], x_at[dx] * 2 + cc) for dz, dx, cc in slab_peers if dz]
-    slab_peers = [(z_at[dz], x_at[dx] * 2 + cc) for dz, dx, cc in slab_peers]
+    flips = sorted(((a, b, k, e) for a in (0, 1) for b in (0, 1) for k in (0, 1) for e in (0, 1)), key=sum)[:0:-1]
+    hops = sorted(
+        ((a, b, k, e) for a in range(4) for b in (0, 1) for k in (0, 1) for e in (0, 1)),
+        key=lambda h: -(min(h[0], 4 - h[0]) + h[1] + h[2] + 0.1 * h[3]),
+    )[:-1]
+    cube_peers, cube_row, cube_col, group_peers, seat, my_kind = [], [], [], [], [], []
+    for h in range(2):
+        zs, ys, xs = (rem(v + h, 4) for v in (z, y, x))
+        zo, yo, xo = (rem(7 - v - h, 4) for v in (zs, ys, xs))
+        long, pair = (zs, xs) if h == 0 else (xs, zs)
+        peers = []
+        for a, b, k, e in flips:
+            zt, yt, xt, ct = (z, zo)[a], (y, yo)[b], (x, xo)[k], (c, 1 - c)[e]
+            lt = rem((zt, xt)[h] + h, 4)
+            col = pl.multiple_of(h * 1536 + (div(lt, 2) * 2 + ct) * 384, 128)
+            peers.append((zt * 32 + yt * 8 + xt * 2 + ct, col))
+        cube_peers.append(peers)
+        at = div(zs, 2) * 128 + div(ys, 2) * 64 + c * 16
+        cube_row.append(pl.multiple_of(at + 32 * jnp.where(kind(xs) == 1, div(xs, 2), 1 - div(xs, 2)), 16))
+        cube_col.append(pl.multiple_of(h * 1536 + (div(long, 2) * 2 + c) * 384, 128))
+        seat.append(((long * 2 + rem(ys, 2)) * 2 + rem(pair, 2)) * 2 + c)
+        my_kind.append((kind(zs) * 2 + kind(ys)) * 2 + kind(xs))
+        peers = []
+        for a, b, k, e in hops:
+            lt, ct = rem(long + a, 4), (c, 1 - c)[e]
+            yt, pt = (ys, ys + 1 - 2 * rem(ys, 2))[b], (pair, pair + 1 - 2 * rem(pair, 2))[k]
+            there = ((lt * 2 + rem(yt, 2)) * 2 + rem(pt, 2)) * 2 + ct
+            zt, xt = (lt, pt) if h == 0 else (pt, lt)
+            which = (kind(zt) * 2 + kind(yt)) * 2 + kind(xt)
+            device = rem(zt + 4 - h, 4) * 32 + rem(yt + 4 - h, 4) * 8 + rem(xt + 4 - h, 4) * 2 + ct
+            peers.append((device, there, which))
+        group_peers.append(peers)
     chips = [z_at[dz] * 16 + y_at[dy] * 4 + x_at[dx] for dz, dy, dx in ALL]
 
     barrier = pltpu.get_barrier_semaphore()
 
     def greet(semaphore, device):
         pl.semaphore_signal(semaphore, inc=1, device_id=(device,), device_id_type=MESH)
-
-    for zt, xt in far_peers:
-        greet(barrier, zt * 32 + y * 8 + xt)
-    for t in plane_peers:
-        greet(barrier, z * 32 + t)
 
     pairs = [
         (hidden_h, hidden), (again_h, again),
@@ -99,7 +123,18 @@
         (gate_h.at[0], gate), (up_h.at[0], up), (down_h.at[0], down), (sg_h, sg), (su_h, su), (sd_h, sd),
     ]
     copies = [pltpu.make_async_copy(src, dst, loc.at[i]) for i, (src, dst) in enumerate(pairs)]
-    for copy in copies:
+    for copy in copies[:5]:
+        copy.start()
+
+    for i, (a, b, k, e) in enumerate(hops):
+        greet(barrier, group_peers[0][i][0])
+        if b:
+            greet(barrier, group_peers[1][i][0])
+    for zt in (z, 3 - z):
+        for xt in (3 - x, 3 - (x + 1 - 2 * rem(x, 2))):
+            for ct in (c, 1 - c):
+                greet(barrier, zt * 32 + y * 8 + xt * 2 + ct)
+    for copy in copies[5:]:
         copy.start()
 
     def ready(lo, hi):
@@ -121,28 +156,41 @@
     ready(0, 2)
     h32 = hidden[...].astype(F32)
     normed = rms(h32, again[...], 1e-6).astype(BF16).astype(F32)
-    for yy in range(4):
-        for zz in range(4):
+    for i in range(2):
+        for b in range(16):
+            lines[i * 16 + b : i * 16 + b + 1, :] = normed[i : i + 1, b * 128 : b * 128 + 128]
+    low = iota((1, 128), 1) < 64
+    turned = [pltpu.roll(lines[...], 32 * i, 1) for i in (1, 2, 3)] + [lines[...]]
+    for h in range(2):
+        for which in range(8):
+            sz, sy, sx = which // 4, which // 2 % 2, which % 2
+            first_half, second_half = turned[h + 2 * sx], turned[(h + 2 - 2 * sx) % 4]
             for i in range(2):
-                at = zz * 512 + yy * 128
-                s1f[yy, i * 4 + zz : i * 4 + zz + 1, :] = normed[i : i + 1, at : at + 128]
+                for zi in range(2):
+                    zz = (((0, 3), (1, 2))[sz][zi] - h) % 4
+                    left_at, right_at = (i * 16 + zz * 4 + (yy - h) % 4 for yy in ((0, 3), (1, 2))[sy])
+                    line = jnp.where(low, first_half[left_at : left_at + 1], second_half[right_at : right_at + 1])
+                    s1f[h, which, i * 2 + zi : i * 2 + zi + 1, :] = line
     s1[...] = s1f[...].astype(BF16)
     for j in range(16):
         hs[j] = h32[:, j * 128 : j * 128 + 128]
     ready(2, 5)
     pl.semaphore_wait(barrier, 55)
 
-    at = pl.multiple_of(slab * 16, 16)
-    for zt, xt in slab_peers:
-        col = pl.multiple_of(xt * 384, 128)
-        remote(wcat.at[:, pl.ds(col, 384)], wbuf.at[pl.ds(at, 16), :], W, zt * 32 + y * 8 + xt).start()
-    for t in plane_peers:
-        remote(s1.at[div(t, 8)], r1.at[plane], P1, z * 32 + t).start()
-    for t in plane_peers:
-        greet(met, z * 32 + t)
-    own = pl.ds(pl.multiple_of(slab * 16, 16), 16)
-    wbuf[own, :] = wcat[:, pl.ds(pl.multiple_of(xc * 384, 128), 384)]
-    r1[plane] = s1[y]
+    for h in range(2):
+        for device, there, which in group_peers[h]:
+            remote(s1.at[h, which], r1.at[h, seat[h]], P1, device).start()
+    for i in range(15):
+        for h in range(2):
+            device, col = cube_peers[h][i]
+            remote(
+                wcat.at[:, pl.ds(col, 384)], wbuf.at[h, pl.ds(cube_row[h], 16), :], W, device
+            ).start()
+    for device, there, which in group_peers[0]:
+        greet(met, device)
+    for h in range(2):
+        wbuf[h, pl.ds(cube_row[h], 16), :] = wcat[:, pl.ds(cube_col[h], 384)]
+        r1[h, seat[h]] = s1[h, my_kind[h]]
     hbuf[q] = hs[q]
 
     ready(5, 8)
@@ -151,16 +199,15 @@
         iota((128, 256), 1) == 4 * (iota((128, 256), 0) // 2) + 2 * c + iota((128, 256), 0) % 2, 1.0, 0.0
     ).astype(BF16)
     before = jnp.where(iota((256, 256), 0) < iota((256, 256), 1), 1.0, 0.0).astype(BF16)
-    picks, back = [], []
+    picks, back, slot_weight = [], [], []
     for i, expert in enumerate((me, mate)):
         hit = routing[...] == expert
         here = jnp.sum(jnp.where(hit, 1.0, 0.0), axis=0, keepdims=True)
         rank = dot(jnp.broadcast_to(here, (16, 256)).astype(BF16), before)[0:1]
         full = jnp.where(rank == iota((SLOTS, 256), 0).astype(F32), here, 0.0)
         back.append(dot_nt(sel, full.astype(BF16)))
-        if i == 0:
-            weight = jnp.sum(jnp.where(hit, rweight[...], 0.0), axis=0, keepdims=True)
-            weight = jnp.sum(full * weight, axis=1, keepdims=True)
+        weight = jnp.sum(jnp.where(hit, rweight[...], 0.0), axis=0, keepdims=True)
+        slot_weight.append(jnp.sum(full * weight, axis=1, keepdims=True))
         mark = (iota((SLOTS, 256), 0) - OWN == iota((SLOTS, 256), 1) - 2 * expert) & (
             iota((SLOTS, 256), 1) // 2 == expert
         )
@@ -169,17 +216,23 @@
     picks = jnp.concatenate(picks, axis=0).astype(BF16)
     back = jnp.concatenate(back, axis=1).astype(BF16)
 
-    arrived(r1.at[pl.ds(0, 31)], P1)
-    x1[...] = r1[...].astype(F32).reshape(256, 128)
-    wide = jnp.concatenate([x1[pl.ds(b, 64, stride=4), :].astype(BF16) for b in range(4)], axis=1)
-    arrived(wbuf.at[pl.ds(0, 496), :], W)
-    part[...] = dot(wide, wbuf[...])
-    for i in range(32):
-        s2[i] = part[2 * i : 2 * i + 2, :]
-
-    for t in plane_peers:
-        remote(s2.at[t], r2.at[plane], P2, z * 32 + t).start()
-    r2[plane] = s2[plane]
+    arrived(r1.at[:, pl.ds(0, 31)], P1)
+    for h in range(2):
+        for i in range(32):
+            x1[h, 4 * i : 4 * i + 4, :] = r1[h, i].astype(F32)
+    arrived(wbuf.at[:, pl.ds(0, 240), :], W)
+    for h in range(2):
+        wide = jnp.concatenate([x1[h, pl.ds(b, 64, stride=2), :].astype(BF16) for b in range(2)], axis=1)
+        part[h] = dot(wide, wbuf[h])
+        for i in range(32):
+            s2[h, i] = part[h, 2 * i : 2 * i + 2, :]
+
+    for i in range(31):
+        for h in range(2):
+            device, there, which = group_peers[h][i]
+            remote(s2.at[h, there], r2.at[h, seat[h]], P2, device).start()
+    for h in range(2):
+        r2[h, seat[h]] = s2[h, seat[h]]
     pl.semaphore_wait(met, 31)
     for t in chips:
         col = pl.multiple_of(rem(t, 16) * 128, 128)
@@ -187,13 +240,18 @@
     for dy, dx in NEAR[:-1]:
         t = y_at[dy] * 4 + x_at[dx]
         remote(hs.at[t], hbuf.at[q], HID, z * 32 + t * 2 + c).start()
-    arrived(r2.at[pl.ds(0, 31)], P2)
+    ready(14, 17)
+    remote(gate, gate_x, GX, mate).start()
+    remote(up, up_x, UX, mate).start()
+    arrived(r2.at[:, pl.ds(0, 31)], P2)
 
     for u in range(24):
-        cb, at = u // 3, (u % 3) * 128
-        val = r2[cb, :, at : at + 128]
-        for yy in range(1, 4):
-            val = val + r2[yy * 8 + cb, :, at : at + 128]
+        at = (u % 3) * 128
+        val = None
+        for src in range(32):
+            if (src // 16) * 2 + src % 2 == u // 3 % 4:
+                term = r2[u // 12, src, :, at : at + 128]
+                val = term if val is None else val + term
         for s in range(2):
             line = val[s : s + 1, :]
             if u < 16:
@@ -269,6 +327,7 @@
     r3[q] = s3[...]
     arrived(obuf.at[pl.ds(0, 63), 0], O)
     remote(obuf.at[:, c], obuf.at[:, c], OX, mate).start()
+    remote(down, down_x, DX, mate).start()
     arrived(hbuf.at[pl.ds(0, 15)], HID)
     for i in range(16):
         hb[2 * i : 2 * i + 2, :] = hbuf[i]
@@ -283,48 +342,49 @@
 
     for t in chips:
         remote(am, gat.at[q, z], P5, t * 2 + c).start()
-    ready(14, 20)
+    ready(17, 20)
     arrived(racc.at[pl.ds(0, CHIPS - 1)], P5)
     for b in range(8):
         cols = jnp.concatenate([gat[2 * b].reshape(128, 128), gat[2 * b + 1].reshape(128, 128)], axis=1)
-        got = dot(picks, cols)
-        mine[:, b * 256 : b * 256 + 256] = got[:SLOTS]
-        theirs[:, b * 256 : b * 256 + 256] = got[SLOTS:].astype(BF16)
-    remote(theirs, picked, PX, mate).start()
-    arrived(picked, PX)
-    mixed = mine[...] + picked[...].astype(F32)
+        mine[:, b * 256 : b * 256 + 256] = dot(picks, cols)
+    arrived(gate_x, GX)
+    arrived(up_x, UX)
+    arrived(down_x, DX)
+    mixed = mine[...]
     moe = rms(mixed, mgain[...], 1e-6).astype(BF16)
-    hid = (jax.nn.silu(dot(moe, gate[...])) * dot(moe, up[...])).astype(BF16)
-    answer = dot(hid, down[...]).astype(BF16).astype(F32) * weight
-    for b in range(8):
-        ans[b, 0:SLOTS] = answer[:, b * 256 : b * 256 + 256].astype(BF16)
-    remote(ans.at[:, pl.ds(0, SLOTS)], ans.at[:, pl.ds(SLOTS, SLOTS)], AX, mate).start()
-    arrived(ans.at[:, pl.ds(0, SLOTS)], AX)
+    for i, (g, u, d) in enumerate(((gate, up, down), (gate_x, up_x, down_x))):
+        rows = moe[i * SLOTS : i * SLOTS + SLOTS]
+        hid = (jax.nn.silu(dot(rows, g[...])) * dot(rows, u[...])).astype(BF16)
+        answer = dot(hid, d[...]).astype(BF16).astype(F32) * slot_weight[i]
+        for b in range(8):
+            ans[b, i * SLOTS : i * SLOTS + SLOTS] = answer[:, b * 256 : b * 256 + 256].astype(BF16)
     for b in range(8):
         tiles = dot(back, ans[b])
         for half in range(2):
             spread[half, pl.ds(b, 128, stride=8), :] = tiles[:, half * 128 : half * 128 + 128]
     for k in (2, 1, 3, 0):
-        lines = pl.ds(pl.multiple_of(z_at[k] * 16, 16), 16)
+        owners = pl.ds(pl.multiple_of(z_at[k] * 16, 16), 16)
         rows = pl.ds(pl.multiple_of(z_at[k] * 256, 256), 256)
         tiles = jnp.concatenate([spread[0, rows, :], spread[1, rows, :]], axis=1)
-        res[lines] = tiles.astype(BF16).reshape(16, 16, 256)
+        res[owners] = tiles.astype(BF16).reshape(16, 16, 256)
         for dy, dx in NEAR if k else NEAR[:-1]:
             t = z_at[k] * 16 + y_at[dy] * 4 + x_at[dx]
             remote(res.at[t], racc.at[chip], P6, t * 2 + c).start()
     racc[chip] = res[chip]
+    moe = moe[:SLOTS]
     hid = (jax.nn.silu(dot(moe, sg[...])) * dot(moe, su[...])).astype(BF16)
     shared = dot(hid[OWN:], sd[...])
-    left(wbuf.at[pl.ds(0, 496), :], W)
+    left(wbuf.at[:, pl.ds(0, 240), :], W)
     left(obuf.at[pl.ds(0, 63), 0], O)
     left(obuf.at[:, 0], OX)
     left(hbuf.at[pl.ds(0, 15)], HID)
-    left(r1.at[pl.ds(0, 31)], P1)
-    left(r2.at[pl.ds(0, 31)], P2)
+    left(r1.at[:, pl.ds(0, 31)], P1)
+    left(r2.at[:, pl.ds(0, 31)], P2)
     left(r3.at[pl.ds(0, 15)], P3)
     left(racc.at[pl.ds(0, CHIPS - 1)], P5)
-    left(picked, PX)
-    left(ans.at[:, pl.ds(0, SLOTS)], AX)
+    left(gate, GX)
+    left(up, UX)
+    left(down, DX)
     arrived(racc.at[pl.ds(0, CHIPS - 1)], P6)
 
     def add(i, carry):
@@ -346,17 +406,18 @@
     scratch = [
         ((2, D), BF16), ((1, 8), F32), ((1, 256), F32), ((1, D), F32), ((1, D), F32),
         ((6, 256), jnp.int32), ((6, 256), F32),
-        ((16, 3072), BF16), ((16, D), BF16), ((512, 384), BF16), ((CHIPS, 2, 16, 128), BF16),
+        ((16, 3072), BF16), ((16, D), BF16), ((2, 256, 384), BF16), ((CHIPS, 2, 16, 128), BF16),
         ((2, CACHE, 512), BF16), ((2, CACHE, 512), BF16),
         ((D, 512), BF16), ((D, 512), BF16), ((512, D), BF16),
         ((D, 512), BF16), ((D, 512), BF16), ((512, D), BF16),
+        ((D, 512), BF16), ((D, 512), BF16), ((512, D), BF16),
         ((16, 2, 128), F32), ((16, 2, 128), F32), ((32, 128), F32),
-        ((4, 8, 128), F32), ((4, 8, 128), BF16), ((32, 8, 128), BF16), ((256, 128), F32), ((64, 384), F32),
-        ((32, 2, 384), F32), ((32, 2, 384), F32),
+        ((32, 128), F32), ((2, 8, 4, 128), F32), ((2, 8, 4, 128), BF16), ((2, 32, 4, 128), BF16), ((2, 128, 128), F32), ((2, 64, 384), F32),
+        ((2, 32, 2, 384), F32), ((2, 32, 2, 384), F32),
         ((2, 16, 128), F32), ((2, 4, 128), F32), ((2, 2, 256), F32),
         ((2, 16, 128), F32), ((2, 16, 128), BF16), ((16, 2, 16, 128), BF16), ((512, 128), F32),
         ((32, 128), BF16), ((16, 4, 32, 128), BF16), ((2, 1024, 128), F32),
-        ((SLOTS, D), F32), ((SLOTS, D), BF16), ((SLOTS, D), BF16),
+        ((2 * SLOTS, D), F32),
         ((8, 2 * SLOTS, 256), BF16), ((CHIPS, 16, 256), BF16), ((CHIPS, 16, 256), BF16), ((2, D), F32),
     ]
     packed = pl.pallas_call(
@@ -366,7 +427,7 @@
         out_specs=pl.BlockSpec(memory_space=pltpu.VMEM),
         scratch_shapes=[pltpu.SMEM((2,), jnp.int32)]
         + [pltpu.VMEM(*s) for s in scratch]
-        + [pltpu.SemaphoreType.DMA((20,)), pltpu.SemaphoreType.DMA((11,)), pltpu.SemaphoreType.DMA((11,))]
+        + [pltpu.SemaphoreType.DMA((20,)), pltpu.SemaphoreType.DMA((12,)), pltpu.SemaphoreType.DMA((12,))]
         + [pltpu.SemaphoreType.REGULAR],
         compiler_params=pltpu.CompilerParams(
             collective_id=0, has_side_effects=True, vmem_limit_bytes=60 * 1024 * 1024

time: 52.4 us -> 49.9 us (0.952)
  Pallas kernels: 51.5 us -> 49 us
    pallas_call x1, Pallas kernels: 50.2 us -> 47.7 us  [on_device(): pl.pallas_call(kernel, out_shape=jax.ShapeDtypeStruct((2, D + 1024), BF16...]
where the time goes in v5:
time: 49.9 us; the launch traced here: 49.6 us
  Pallas kernels  49 us (98%)
  between operations  0.65 us (1%)
    pallas_call x1, Pallas kernels, on_device(): pl.pallas_call(kernel, out_shape=jax.ShapeDtypeStruct((2, D + 1024), BF16...  47.7 us
    pallas_call x1, Pallas kernels, on_device(): pl.pallas_call(unpack, out_shape=(jax.ShapeDtypeStruct((2, D), BF16), jax...  1.31 us

profile of v5, /device:TPU:0, one launch (start us, length us, event | category | flops | bytes accessed | tf_op | source)
XLA Modules:
  0.0 49.6 jit_solution(5193423686316774353)
XLA Ops:
  0.6 47.7 %shard_map.211.src = bf16[2,3072]{1,0:T(2,128)(2,1)} custom-call(s32[2]{0:T(128)} %lengths_h.1, bf16[2,2048]{1,0:T(2,128)(2,1)} %hidden_h.1, f32[1,8]{1,0:T(1,128)} %bitcast.11, f32[1,256]{1,0:T(1,128)} %bitcast.10, f32[1,2048]{1,0:T(1,128)} %bitcast.6, f32[1,2048]{1,0:T(1,128)} %bitcast.7, s32[6,256]{1,0:T(8,128)} %bitcast.8, f32[6,256]{1,0:T(8,128)} %bitcast.9, ...), custom_call_target="tpu_custom_call" | custom-call | tf_op jit(solution)/shard_map/pallas_call | solution.py:423
  48.3 1.3 %shard_map.212 = (bf16[2,2048]{1,0:T(2,128)(2,1)}, bf16[2,512]{1,0:T(2,128)(2,1)}, bf16[2,512]{1,0:T(2,128)(2,1)}) custom-call(bf16[2,3072]{1,0:T(2,128)(2,1)} %shard_map.211.src), custom_call_target="tpu_custom_call" | custom-call | tf_op jit(solution)/shard_map/pallas_call | solution.py:448

commit v6 on v5

--- a/solution.py
+++ b/solution.py
@@ -14,7 +14,7 @@
 CACHE = 1024
 SLOTS = 32
 OWN = 24
-W, O, OX, HID, P1, P2, P3, P5, GX, UX, DX, P6 = range(12)
+W, O, OX, HID, P1, P2, P3, GX, UX, DX, P6, P5 = range(12)
 
 
 def dot(a, b):
@@ -59,8 +59,8 @@
     out,
     lengths, hidden, lam, hgain, again, mgain, routing, rweight,
     wcat, obuf_s, wbuf, obuf, kc, vc, gate, up, down, gate_x, up_x, down_x, sg, su, sd,
-    hs, hbuf, hb, lines, s1f, s1, r1, x1, part, s2, r2, qscr, kscr, vscr, at16, s3, r3, x3,
-    am, gat, spread, mine, ans, res, racc, fin,
+    hs, hbuf, hb, lines, s1f, s1, r1, x1, part, s2, r2, angles, qscr, kscr, vscr, at16, s3, r3, x3,
+    am, gat, spread, mine, pre, ans, res, racc, fin,
     loc, snd, rcv, met,
 ):
     me = lax.axis_index("ep")
@@ -216,6 +216,14 @@
     picks = jnp.concatenate(picks, axis=0).astype(BF16)
     back = jnp.concatenate(back, axis=1).astype(BF16)
 
+    ready(8, 14)
+    lane = iota((1, 128), 1)
+    inverse = jnp.exp((lane % 64).astype(F32) * (-13.122363377404328 / 64))
+    for s in range(2):
+        angle = lengths[s].astype(F32) * inverse
+        angles[0, s : s + 1, :] = jnp.cos(angle)
+        angles[1, s : s + 1, :] = jnp.where(lane < 64, -jnp.sin(angle), jnp.sin(angle))
+
     arrived(r1.at[:, pl.ds(0, 31)], P1)
     for h in range(2):
         for i in range(32):
@@ -263,25 +271,18 @@
                 v = u - 20
                 vscr[s, v // 2 : v // 2 + 1, (v % 2) * 128 : (v % 2) * 128 + 128] = line
 
-    ready(8, 14)
     rows = iota((16, 1), 0)
     pair_of = (rows // 8) + 2 * ((rows % 8) // 4)
     first = iota((8, 1), 0) < 4
     lam_col = jnp.sum(jnp.where(iota((8, 8), 0) == iota((8, 8), 1), lam[...], 0.0), axis=1, keepdims=True)
     scale = 128 ** (-0.5)
-    place = iota((1, CACHE), 1)
-    lane = iota((1, 128), 1)
-    inverse = jnp.exp((lane % 64).astype(F32) * (-13.122363377404328 / 64))
 
     def turn(v, cos_row, sin_row):
         return (v * cos_row + pltpu.roll(v, 64, 1) * sin_row).astype(BF16)
 
     q_rows, k_rows, v_rows, all_scores = [], [], [], []
     for s in range(2):
-        angle = lengths[s].astype(F32) * inverse
-        cos_row = jnp.cos(angle)
-        sin_row = jnp.sin(angle)
-        sin_row = jnp.where(lane < 64, -sin_row, sin_row)
+        cos_row, sin_row = angles[0, s : s + 1, :], angles[1, s : s + 1, :]
         qq = turn(qscr[s], cos_row, sin_row).astype(F32)
         wide = jnp.concatenate([jnp.where(pair_of == u, qq, 0.0) for u in range(4)], axis=1).astype(BF16)
         all_scores.append(dot_nt(wide, kc[s]))
@@ -302,7 +303,7 @@
             pair_of == 0, kn[0:1], jnp.where(pair_of == 1, kn[1:2], jnp.where(pair_of == 2, kn[2:3], kn[3:4]))
         )
         own_score = jnp.sum(qq * k_of, axis=1, keepdims=True) * scale
-        live = place < lengths[s]
+        live = iota((1, CACHE), 1) < lengths[s]
         peak = jnp.maximum(jnp.max(jnp.where(live, scores, -jnp.inf), axis=1, keepdims=True), own_score)
         weights = jnp.where(live, jnp.exp(scores - peak), 0.0)
         own_weight = jnp.exp(own_score - peak)
@@ -340,21 +341,36 @@
     am[...] = mixed
     gat[q, z] = mixed
 
-    for t in chips:
-        remote(am, gat.at[q, z], P5, t * 2 + c).start()
+    for dy in (2, 1, 3, 0):
+        for dz, dx in NEAR if dy else NEAR[:-1]:
+            t = z_at[dz] * 16 + y_at[dy] * 4 + x_at[dx]
+            remote(am, gat.at[q, z], P5 + dy, t * 2 + c).start()
     ready(17, 20)
-    arrived(racc.at[pl.ds(0, CHIPS - 1)], P5)
-    for b in range(8):
-        cols = jnp.concatenate([gat[2 * b].reshape(128, 128), gat[2 * b + 1].reshape(128, 128)], axis=1)
-        mine[:, b * 256 : b * 256 + 256] = dot(picks, cols)
-    arrived(gate_x, GX)
-    arrived(up_x, UX)
-    arrived(down_x, DX)
-    mixed = mine[...]
-    moe = rms(mixed, mgain[...], 1e-6).astype(BF16)
-    for i, (g, u, d) in enumerate(((gate, up, down), (gate_x, up_x, down_x))):
-        rows = moe[i * SLOTS : i * SLOTS + SLOTS]
-        hid = (jax.nn.silu(dot(rows, g[...])) * dot(rows, u[...])).astype(BF16)
+    squares = jnp.zeros((2 * SLOTS, 1), F32)
+    for k, dy in enumerate((2, 1, 3, 0)):
+        arrived(racc.at[pl.ds(0, 16 if dy else 15)], P5 + dy)
+        if k == 0:
+            arrived(gate_x, GX)
+            arrived(up_x, UX)
+            arrived(down_x, DX)
+        ys = y_at[4 - dy if dy else 0]
+        at = pl.multiple_of(ys * 512, 512)
+        tiles = [gat[ys * 4 + i].reshape(128, 128) for i in range(4)]
+        got = jnp.concatenate(
+            [dot(picks, jnp.concatenate(tiles[i : i + 2], axis=1)) for i in (0, 2)], axis=1
+        )
+        mine[:, pl.ds(at, 512)] = got[OWN:SLOTS]
+        squares = squares + jnp.sum(got * got, axis=1, keepdims=True)
+        got = (got * mgain[:, pl.ds(at, 512)]).astype(BF16)
+        for i, (g, u) in enumerate(((gate, up), (gate_x, up_x))):
+            rows = got[i * SLOTS : i * SLOTS + SLOTS]
+            for j, w in enumerate((g, u)):
+                term = dot(rows, w[pl.ds(at, 512), :])
+                pre[i, j] = term if k == 0 else pre[i, j] + term
+    factor = lax.rsqrt(squares / D + 1e-6)
+    for i, d in enumerate((down, down_x)):
+        f = factor[i * SLOTS : i * SLOTS + SLOTS]
+        hid = (jax.nn.silu(pre[i, 0] * f) * (pre[i, 1] * f)).astype(BF16)
         answer = dot(hid, d[...]).astype(BF16).astype(F32) * slot_weight[i]
         for b in range(8):
             ans[b, i * SLOTS : i * SLOTS + SLOTS] = answer[:, b * 256 : b * 256 + 256].astype(BF16)
@@ -371,9 +387,10 @@
             t = z_at[k] * 16 + y_at[dy] * 4 + x_at[dx]
             remote(res.at[t], racc.at[chip], P6, t * 2 + c).start()
     racc[chip] = res[chip]
-    moe = moe[:SLOTS]
+    mixed = mine[...]
+    moe = rms(mixed, mgain[...], 1e-6).astype(BF16)
     hid = (jax.nn.silu(dot(moe, sg[...])) * dot(moe, su[...])).astype(BF16)
-    shared = dot(hid[OWN:], sd[...])
+    shared = dot(hid, sd[...])
     left(wbuf.at[:, pl.ds(0, 240), :], W)
     left(obuf.at[pl.ds(0, 63), 0], O)
     left(obuf.at[:, 0], OX)
@@ -381,7 +398,8 @@
     left(r1.at[:, pl.ds(0, 31)], P1)
     left(r2.at[:, pl.ds(0, 31)], P2)
     left(r3.at[pl.ds(0, 15)], P3)
-    left(racc.at[pl.ds(0, CHIPS - 1)], P5)
+    for dy in range(4):
+        left(racc.at[pl.ds(0, 16 if dy else 15)], P5 + dy)
     left(gate, GX)
     left(up, UX)
     left(down, DX)
@@ -394,7 +412,7 @@
     for s in range(2):
         for b in range(8):
             fin[s : s + 1, b * 256 : b * 256 + 256] = total[s * 8 + b : s * 8 + b + 1]
-    out[:, 0:D] = (mixed[OWN : OWN + 2] + fin[...] + shared[0:2]).astype(BF16)
+    out[:, 0:D] = (mixed[0:2] + fin[...] + shared[0:2]).astype(BF16)
     left(racc.at[pl.ds(0, CHIPS - 1)], P6)
 
 
@@ -414,10 +432,10 @@
         ((16, 2, 128), F32), ((16, 2, 128), F32), ((32, 128), F32),
         ((32, 128), F32), ((2, 8, 4, 128), F32), ((2, 8, 4, 128), BF16), ((2, 32, 4, 128), BF16), ((2, 128, 128), F32), ((2, 64, 384), F32),
         ((2, 32, 2, 384), F32), ((2, 32, 2, 384), F32),
-        ((2, 16, 128), F32), ((2, 4, 128), F32), ((2, 2, 256), F32),
+        ((2, 2, 128), F32), ((2, 16, 128), F32), ((2, 4, 128), F32), ((2, 2, 256), F32),
         ((2, 16, 128), F32), ((2, 16, 128), BF16), ((16, 2, 16, 128), BF16), ((512, 128), F32),
         ((32, 128), BF16), ((16, 4, 32, 128), BF16), ((2, 1024, 128), F32),
-        ((2 * SLOTS, D), F32),
+        ((SLOTS - OWN, D), F32), ((2, 2, SLOTS, 512), F32),
         ((8, 2 * SLOTS, 256), BF16), ((CHIPS, 16, 256), BF16), ((CHIPS, 16, 256), BF16), ((2, D), F32),
     ]
     packed = pl.pallas_call(
@@ -427,7 +445,7 @@
         out_specs=pl.BlockSpec(memory_space=pltpu.VMEM),
         scratch_shapes=[pltpu.SMEM((2,), jnp.int32)]
         + [pltpu.VMEM(*s) for s in scratch]
-        + [pltpu.SemaphoreType.DMA((20,)), pltpu.SemaphoreType.DMA((12,)), pltpu.SemaphoreType.DMA((12,))]
+        + [pltpu.SemaphoreType.DMA((20,)), pltpu.SemaphoreType.DMA((15,)), pltpu.SemaphoreType.DMA((15,))]
         + [pltpu.SemaphoreType.REGULAR],
         compiler_params=pltpu.CompilerParams(
             collective_id=0, has_side_effects=True, vmem_limit_bytes=60 * 1024 * 1024

time: 49.9 us -> 48.4 us (0.970)
  Pallas kernels: 49 us -> 47.5 us
    pallas_call x1, Pallas kernels: 47.7 us -> 46.2 us  [on_device(): pl.pallas_call(kernel, out_shape=jax.ShapeDtypeStruct((2, D + 1024), BF16...]
where the time goes in v6:
time: 48.4 us; the launch traced here: 48.2 us
  Pallas kernels  47.5 us (98%)
  between operations  0.65 us (1%)
    pallas_call x1, Pallas kernels, on_device(): pl.pallas_call(kernel, out_shape=jax.ShapeDtypeStruct((2, D + 1024), BF16...  46.2 us
    pallas_call x1, Pallas kernels, on_device(): pl.pallas_call(unpack, out_shape=(jax.ShapeDtypeStruct((2, D), BF16), jax...  1.31 us

profile of v6, /device:TPU:0, one launch (start us, length us, event | category | flops | bytes accessed | tf_op | source)
XLA Modules:
  0.0 48.2 jit_solution(10241703357380255776)
XLA Ops:
  0.6 46.2 %shard_map.211.src = bf16[2,3072]{1,0:T(2,128)(2,1)} custom-call(s32[2]{0:T(128)} %lengths_h.1, bf16[2,2048]{1,0:T(2,128)(2,1)} %hidden_h.1, f32[1,8]{1,0:T(1,128)} %bitcast.11, f32[1,256]{1,0:T(1,128)} %bitcast.10, f32[1,2048]{1,0:T(1,128)} %bitcast.6, f32[1,2048]{1,0:T(1,128)} %bitcast.7, s32[6,256]{1,0:T(8,128)} %bitcast.8, f32[6,256]{1,0:T(8,128)} %bitcast.9, ...), custom_call_target="tpu_custom_call" | custom-call | tf_op jit(solution)/shard_map/pallas_call | solution.py:441
  46.9 1.3 %shard_map.212 = (bf16[2,2048]{1,0:T(2,128)(2,1)}, bf16[2,512]{1,0:T(2,128)(2,1)}, bf16[2,512]{1,0:T(2,128)(2,1)}) custom-call(bf16[2,3072]{1,0:T(2,128)(2,1)} %shard_map.211.src), custom_call_target="tpu_custom_call" | custom-call | tf_op jit(solution)/shard_map/pallas_call | solution.py:466

commit v7 on v6

--- a/solution.py
+++ b/solution.py
@@ -216,6 +216,9 @@
     picks = jnp.concatenate(picks, axis=0).astype(BF16)
     back = jnp.concatenate(back, axis=1).astype(BF16)
 
+    ready(14, 17)
+    remote(gate, gate_x, GX, mate).start()
+    remote(up, up_x, UX, mate).start()
     ready(8, 14)
     lane = iota((1, 128), 1)
     inverse = jnp.exp((lane % 64).astype(F32) * (-13.122363377404328 / 64))
@@ -248,9 +251,7 @@
     for dy, dx in NEAR[:-1]:
         t = y_at[dy] * 4 + x_at[dx]
         remote(hs.at[t], hbuf.at[q], HID, z * 32 + t * 2 + c).start()
-    ready(14, 17)
-    remote(gate, gate_x, GX, mate).start()
-    remote(up, up_x, UX, mate).start()
+    remote(down, down_x, DX, mate).start()
     arrived(r2.at[:, pl.ds(0, 31)], P2)
 
     for u in range(24):
@@ -328,7 +329,6 @@
     r3[q] = s3[...]
     arrived(obuf.at[pl.ds(0, 63), 0], O)
     remote(obuf.at[:, c], obuf.at[:, c], OX, mate).start()
-    remote(down, down_x, DX, mate).start()
     arrived(hbuf.at[pl.ds(0, 15)], HID)
     for i in range(16):
         hb[2 * i : 2 * i + 2, :] = hbuf[i]

time: 48.4 us -> 48.4 us (level)
  no operation moved by 1% of the time
where the time goes in v7:
time: 48.4 us; the launch traced here: 48.2 us
  Pallas kernels  47.5 us (98%)
  between operations  0.65 us (1%)
    pallas_call x1, Pallas kernels, on_device(): pl.pallas_call(kernel, out_shape=jax.ShapeDtypeStruct((2, D + 1024), BF16...  46.2 us
    pallas_call x1, Pallas kernels, on_device(): pl.pallas_call(unpack, out_shape=(jax.ShapeDtypeStruct((2, D), BF16), jax...  1.31 us

profile of v7, /device:TPU:0, one launch (start us, length us, event | category | flops | bytes accessed | tf_op | source)
XLA Modules:
  0.0 48.2 jit_solution(16638754074055791300)
XLA Ops:
  0.6 46.2 %shard_map.211.src = bf16[2,3072]{1,0:T(2,128)(2,1)} custom-call(s32[2]{0:T(128)} %lengths_h.1, bf16[2,2048]{1,0:T(2,128)(2,1)} %hidden_h.1, f32[1,8]{1,0:T(1,128)} %bitcast.11, f32[1,256]{1,0:T(1,128)} %bitcast.10, f32[1,2048]{1,0:T(1,128)} %bitcast.6, f32[1,2048]{1,0:T(1,128)} %bitcast.7, s32[6,256]{1,0:T(8,128)} %bitcast.8, f32[6,256]{1,0:T(8,128)} %bitcast.9, ...), custom_call_target="tpu_custom_call" | custom-call | tf_op jit(solution)/shard_map/pallas_call | solution.py:441
  46.9 1.3 %shard_map.212 = (bf16[2,2048]{1,0:T(2,128)(2,1)}, bf16[2,512]{1,0:T(2,128)(2,1)}, bf16[2,512]{1,0:T(2,128)(2,1)}) custom-call(bf16[2,3072]{1,0:T(2,128)(2,1)} %shard_map.211.src), custom_call_target="tpu_custom_call" | custom-call | tf_op jit(solution)/shard_map/pallas_call | solution.py:466
